TPU v7x, 256 devices: a whole 4x4x8 slice. The times are simulated.
256 devices in a mesh: ep: 128 (over z, y, x), tp: 2 (over core).
Axes of the slice: x: 4, y: 4, z: 8, core: 2. Of those that a mesh axis runs over, the one named last changes fastest.
Arguments:
- tokens: bfloat16 [2048, 1024], P('ep'), may hold values from -6 to 6
- mixer_gain: float32 [1024], replicated, may hold values from 0.1 to 1.9
- query_weight: bfloat16 [1024, 1024], P(None, 'tp'), may hold values from -0.1875 to 0.1875
- key_weight: bfloat16 [1024, 256], P(None, 'tp'), may hold values from -0.1875 to 0.1875
- value_weight: bfloat16 [1024, 256], P(None, 'tp'), may hold values from -0.1875 to 0.1875
- head_lambda: float32 [8], P('tp'), may hold values from 0.3 to 0.8
- head_gain: float32 [128], replicated, may hold values from 0.1 to 1.9
- out_weight: bfloat16 [1024, 1024], P('tp'), may hold values from -0.1875 to 0.1875
- cache_keys: bfloat16 [2048, 1024, 256], P('ep', None, 'tp'), may hold values from -700 to 700
- cache_values: bfloat16 [2048, 1024, 256], P('ep', None, 'tp'), may hold values from -6 to 6
- seq_lengths: int32 [2048], P('ep'), may hold values from 2 to 1024, as said below
- channel_gain: float32 [1024], replicated, may hold values from 0.1 to 1.9
- expert_ids: int32 [2048, 6], P('ep'), may hold values from 0 to 127, all different within a row; in each aligned block of 16 rows (0 to 15, 16 to 31, ...) at most 2 rows name the same one
- expert_shares: bfloat16 [2048, 6], P('ep'), may hold values from 0.19921875 to 1
- expert_gate: bfloat16 [128, 1024, 256], P('ep', None, 'tp'), may hold values from -0.1875 to 0.1875
- expert_up: bfloat16 [128, 1024, 256], P('ep', None, 'tp'), may hold values from -0.1875 to 0.1875
- expert_down: bfloat16 [128, 256, 1024], P('ep', 'tp'), may hold values from -0.375 to 0.375
- dense_gate: bfloat16 [1024, 4096], P('tp', 'ep'), may hold values from -0.1875 to 0.1875
- dense_up: bfloat16 [1024, 4096], P('tp', 'ep'), may hold values from -0.1875 to 0.1875
- dense_down: bfloat16 [4096, 1024], P('ep', 'tp'), may hold values from -0.1875 to 0.1875
- branch_gate: float32 [1024], replicated, may hold values from -0.1875 to 0.1875
Outputs:
- layer_out: bfloat16 [2048, 1024], P('ep', 'tp')
Inputs may be any that keep to these rules, and one draw needn't show every extreme that they name: `expert_ids`: each row names 6 different experts; among the 16 rows of one index of ep no expert is named by more than 2 rows. `seq_lengths`: some sequence has all 1024 positions live.
All inputs are finite; a program needn't handle non-finite values.
Results may differ from a plain program's by a relative error of at most 0.017.
The roundings to bfloat16 on the way count: a program that leaves them out, or rounds other values in their place, can miss the bound.
Values may be sent and summed in bfloat16 or wider, within the bound.
No kernel may reach another device: no remote copies, remote signals or barrier semaphores. Data moves between devices by JAX's collectives and lax.ppermute only.
A program may use at most 64 MiB of HBM per device.

v0:
```python
import jax
import jax.numpy as jnp
from jax import lax
from jax.sharding import Mesh
from jax.sharding import PartitionSpec as P

HD = 64
EP = ("ep_0", "ep_1", "ep_2")


NORM_EPS = 1e-06
HEAD_EPS = 1e-05
THETA = 500000.0
LAMBDA_BASE = 0.2


def split_up(shard, dim, devices):
    before, after = (shard.shape[:dim], shard.shape[dim + 1 :])
    return jnp.moveaxis(shard.reshape(*before, devices, -1, *after), dim, 0)


def sum_at_owner(shard, axis, dim):
    devices = lax.axis_size(axis)
    tiles = lax.all_to_all(split_up(shard, dim, devices), axis, 0, 0, tiled=True)
    return jnp.sum(tiles.astype(jnp.float32), axis=0)


def from_everyone(shard, axis):
    devices = lax.axis_size(axis)
    return lax.all_to_all(
        jnp.broadcast_to(shard[None], (devices, *shard.shape)), axis, 0, 0, tiled=True
    )


def of_everyone(shard, axis):
    return from_everyone(shard, axis).astype(jnp.float32).sum(axis=0)


def joined_along(tiles, dim):
    tiles = jnp.moveaxis(tiles, 0, dim)
    shape = tiles.shape
    return tiles.reshape(*shape[:dim], shape[dim] * shape[dim + 1], *shape[dim + 2 :])


def gather_axes(shard, axes, dim):
    far, near = axes
    initial = from_everyone(shard, far)
    tiles = jnp.swapaxes(from_everyone(initial, near), 0, 1)
    return joined_along(tiles.reshape(-1, *shard.shape), dim)


def scatter_axes(shard, axes, dim):
    for axis in axes:
        shard = lax.psum_scatter(shard, axis, scatter_dimension=dim, tiled=True)
    return shard


def norm_rows(values, gain_vec, epsilon):
    mean_square = jnp.mean(values * values, axis=-1, keepdims=True)
    return values * lax.rsqrt(mean_square + epsilon) * gain_vec


def rotate(values, position):
    half_dim = HD // 2
    frequency = THETA ** (-jnp.arange(half_dim, dtype=jnp.float32) * (2.0 / HD))
    angles = position.astype(jnp.float32)[:, None] * frequency[None, :]
    cos_vals = jnp.cos(angles)[:, None, :]
    sin_vals = jnp.sin(angles)[:, None, :]
    first_half = values[..., :half_dim]
    second = values[..., half_dim:]
    return jnp.concatenate(
        [first_half * cos_vals - second * sin_vals, second * cos_vals + first_half * sin_vals],
        axis=-1,
    )


def expert_rows(arrived, expert_gate, expert_up, expert_down):
    source_count, slot_count, model_width = arrived.shape
    stacked = arrived.reshape(source_count * slot_count, model_width)
    gate_part = jnp.dot(stacked, expert_gate[0], preferred_element_type=jnp.float32)
    up_part = jnp.dot(stacked, expert_up[0], preferred_element_type=jnp.float32)
    expert_hidden = (jax.nn.silu(gate_part) * up_part).astype(jnp.bfloat16)
    partial_value = jnp.dot(expert_hidden, expert_down[0], preferred_element_type=jnp.float32)
    partial_value = partial_value.reshape(source_count, slot_count, model_width)
    return sum_at_owner(partial_value.astype(jnp.bfloat16), "tp", 2).astype(jnp.bfloat16)


def dense_branch(partials, dense_down):
    summed = of_everyone(partials.astype(jnp.bfloat16), "tp").astype(jnp.float32)
    unit_count = partials.shape[1] // 2
    dense_hidden = (jax.nn.silu(summed[:, :unit_count]) * summed[:, unit_count:]).astype(
        jnp.bfloat16
    )
    return jnp.dot(dense_hidden, dense_down, preferred_element_type=jnp.float32)


def shards(
    tokens,
    mixer_gain,
    query_weight,
    key_weight,
    value_weight,
    head_lambda,
    head_gain,
    out_weight,
    cache_keys,
    cache_values,
    seq_lengths,
    channel_gain,
    expert_ids,
    expert_shares,
    expert_gate,
    expert_up,
    expert_down,
    dense_gate,
    dense_up,
    dense_down,
    branch_gate,
):
    seq_count, model_width = tokens.shape
    resid = tokens.astype(jnp.float32)
    normed = norm_rows(resid, mixer_gain, NORM_EPS).astype(jnp.bfloat16)
    value_width = 2 * HD
    groups = cache_values.shape[2] // value_width
    local_heads = head_lambda.shape[0]
    per_group = local_heads // groups
    cache_span = cache_keys.shape[1]
    query_raw = jnp.dot(normed, query_weight, preferred_element_type=jnp.float32).reshape(
        seq_count, local_heads * 2, HD
    )
    key_raw = jnp.dot(normed, key_weight, preferred_element_type=jnp.float32).reshape(
        seq_count, groups * 2, HD
    )
    value_new = jnp.dot(normed, value_weight, preferred_element_type=jnp.float32).astype(
        jnp.bfloat16
    )
    value_new = value_new.reshape(seq_count, groups, value_width)
    query = (
        rotate(query_raw, seq_lengths)
        .astype(jnp.bfloat16)
        .reshape(seq_count, groups, per_group, 2, HD)
    )
    key_new = rotate(key_raw, seq_lengths).astype(jnp.bfloat16).reshape(seq_count, groups, 2, HD)
    key_rows = cache_keys.reshape(seq_count, cache_span, groups, 2, HD)
    value_rows = cache_values.reshape(seq_count, cache_span, groups, value_width)
    lambdas = head_lambda.reshape(groups, per_group)
    score_scale = HD ** (-0.5)
    scores = (
        jnp.einsum("sgjcd,slgcd->sgjcl", query, key_rows, preferred_element_type=jnp.float32)
        * score_scale
    )
    fresh_score = (
        jnp.einsum("sgjcd,sgcd->sgjc", query, key_new, preferred_element_type=jnp.float32)
        * score_scale
    )
    live = jnp.arange(cache_span)[None, :] < seq_lengths[:, None]
    scores = jnp.where(live[:, None, None, None, :], scores, -jnp.inf)
    peak = jnp.maximum(jnp.max(scores, axis=-1), fresh_score)
    expo_scores = jnp.exp(scores - peak[..., None])
    expo_fresh = jnp.exp(fresh_score - peak)
    denom_sum = jnp.sum(expo_scores, axis=-1) + expo_fresh
    probability = expo_scores / denom_sum[..., None]
    prob_fresh = expo_fresh / denom_sum
    weight = (probability[:, :, :, 0] - lambdas[None, :, :, None] * probability[:, :, :, 1]).astype(
        jnp.bfloat16
    )
    weight_fresh = (prob_fresh[..., 0] - lambdas[None] * prob_fresh[..., 1]).astype(jnp.bfloat16)
    head_mix = jnp.einsum("sgjl,slgv->sgjv", weight, value_rows, preferred_element_type=jnp.float32)
    head_mix = (
        head_mix
        + weight_fresh.astype(jnp.float32)[..., None] * value_new.astype(jnp.float32)[:, :, None, :]
    )
    head_mix = head_mix.reshape(seq_count, local_heads, value_width)
    head_out = (norm_rows(head_mix, head_gain, HEAD_EPS) * (1.0 - LAMBDA_BASE)).astype(jnp.bfloat16)
    attn_part = jnp.dot(
        head_out.reshape(seq_count, local_heads * value_width),
        out_weight,
        preferred_element_type=jnp.float32,
    )
    attn_sum = of_everyone(attn_part.astype(jnp.bfloat16), "tp").astype(jnp.float32)
    resid_mid = (resid + attn_sum).astype(jnp.bfloat16)
    ffn_input = norm_rows(resid_mid.astype(jnp.float32), channel_gain, NORM_EPS).astype(
        jnp.bfloat16
    )
    gate_own = jax.nn.sigmoid(
        jnp.dot(ffn_input.astype(jnp.float32), branch_gate, precision=lax.Precision.HIGHEST)
    )
    half_width = model_width // lax.axis_size("tp")
    offset = lax.axis_index("tp") * half_width
    mid_half = lax.dynamic_slice_in_dim(resid_mid, offset, half_width, 1)
    experts_total = lax.axis_size(EP)
    top_count = expert_ids.shape[1]
    capacity = max(2, 2 * seq_count * top_count // experts_total)
    slot_ids = jnp.arange(1, capacity + 1, dtype=jnp.int32)
    named_mask = expert_ids[:, :, None] == jnp.arange(experts_total, dtype=jnp.int32)[None, None, :]
    picked = jnp.any(named_mask, axis=1)
    share_wide = expert_shares.astype(jnp.float32)[:, :, None]
    row_share = jnp.sum(jnp.where(named_mask, share_wide, jnp.zeros_like(share_wide)), axis=1)
    slot_rank = jnp.cumsum(picked.astype(jnp.int32), axis=0)
    placed = picked[None, :, :] & (slot_rank[None, :, :] == slot_ids[:, None, None])
    outgoing = jnp.einsum(
        "cse,sd->ecd", placed.astype(jnp.bfloat16), ffn_input, preferred_element_type=jnp.float32
    ).astype(jnp.bfloat16)
    expert_out = expert_rows(
        lax.all_to_all(outgoing, EP, split_axis=0, concat_axis=0, tiled=True),
        expert_gate,
        expert_up,
        expert_down,
    )
    returned = lax.all_to_all(expert_out, EP, split_axis=0, concat_axis=0, tiled=True)
    routed_sum = jnp.einsum(
        "cse,ecd->sd",
        placed.astype(jnp.float32) * row_share[None],
        returned.astype(jnp.float32),
        precision=lax.Precision.HIGHEST,
    )
    input_half = lax.dynamic_slice_in_dim(ffn_input, offset, half_width, 1)
    piece_rows = gather_axes(input_half, ("ep_0", ("ep_1", "ep_2")), 0)
    partials = jnp.concatenate(
        [
            jnp.dot(piece_rows, dense_gate, preferred_element_type=jnp.float32),
            jnp.dot(piece_rows, dense_up, preferred_element_type=jnp.float32),
        ],
        axis=1,
    )
    branch_term = dense_branch(partials, dense_down)
    summed = scatter_axes(branch_term, EP, 0)
    summed = gate_own[:, None] * summed + routed_sum
    return (mid_half.astype(jnp.float32) + summed).astype(jnp.bfloat16)


def solution(mesh):
    torus = Mesh(mesh.devices.reshape(8, 4, 4, mesh.shape["tp"]), ("ep_0", "ep_1", "ep_2", "tp"))
    return jax.shard_map(
        shards,
        mesh=torus,
        in_specs=(
            P(EP, None),
            P(),
            P(None, "tp"),
            P(None, "tp"),
            P(None, "tp"),
            P("tp"),
            P(),
            P("tp", None),
            P(EP, None, "tp"),
            P(EP, None, "tp"),
            P(EP),
            P(),
            P(EP, None),
            P(EP, None),
            P(EP, None, "tp"),
            P(EP, None, "tp"),
            P(EP, "tp", None),
            P("tp", EP),
            P("tp", EP),
            P(EP, "tp"),
            P(),
        ),
        out_specs=P(EP, "tp"),
        check_vma=False,
    )
```

profile of v0, /device:TPU:1, one launch (start us, length us, event | category | flops | bytes accessed | tf_op | source)
XLA Modules:
  0.0 212.5 jit_solution(14512335145991299571)
XLA Ops:
  6.5 0.7 convert_element_type.106
  7.3 0.7 iota_compare_fusion
  8.0 0.9 fusion.32
  8.9 1.2 fusion.67
  10.1 0.1 reshape.240
  10.2 1.6 fusion.69
  11.8 0.1 reshape.238
  11.8 0.1 fusion.72
  11.9 0.1 multiply_cosine_fusion
  12.0 0.1 subtract_convert_fusion.1
  12.2 0.1 maximum_bitcast_fusion
  12.3 0.2 fusion.45
  12.5 0.1 copy.100
  12.6 6.4 %copy.86 = bf16[16,1024,128]{1,2,0:T(8,128)(2,1)} copy(bf16[16,1024,128]{2,1,0:T(8,128)(2,1)} %param.29) | data formatting | bytes 8388608 | tf_op args[8]
  19.1 3.0 %fusion.73 = (f32[16,4,2]{1,2,0:T(2,128)S(1)}, f32[16,1,4,2,1024]{4,2,3,0,1:T(4,128)S(1)}) fusion(bf16[16,1024,2,64]{1,3,2,0:T(8,128)(2,1)} %bitcast.161, bf16[16,4,2,32]{3,1,2,0:T(4,128)(2,1)S(1)} %copy.85, bf16[16,4,2,32]{3,1,2,0:T(4,128)(2,1)S(1)} %copy.84, pred[16,1024]{1,0:T(8,128)(4,1)S(1)} %iota_compare_fusion), kind=kOutput, calls=%fused_computation.117 | convolution fusion | flops 17203072 | bytes 4751872 | tf_op jit(solution)/shard_map/sgjcd,slgcd->sgjcl/dot_general | solution.py:149
  22.1 0.1 copy.87
  22.2 0.1 copy.88
  22.3 0.3 fusion.14
  22.7 0.1 copy.89
  22.8 0.1 copy.90
  22.9 0.3 fusion.13
  23.2 0.1 fusion.62
  23.3 0.1 copy.92
  23.4 0.2 fusion.8
  23.6 3.0 %multiply_reduce_fusion = (f32[16,4]{1,0:T(8,128)S(1)}, f32[16,4,128]{2,1,0:T(4,128)S(1)}) fusion(f32[16,128]{1,0:T(8,128)S(1)} %fusion.8, f32[16,4]{1,0:T(8,128)S(1)} %copy.92, bf16[16,1024,128]{2,1,0:T(8,128)(2,1)} %param.30, f32[16,1,4,2,1024]{4,2,3,0,1:T(4,128)S(1)} %fusion.13, f32[4]{0:T(128)S(1)} %copy-done.10), kind=kOutput, calls=%fused_computation.70 | convolution fusion | flops 17006528 | bytes 4760080 | tf_op jit(solution)/shard_map/sgjl,slgv->sgjv/dot_general | solution.py:168
  26.6 0.1 broadcast_multiply_fusion
  26.7 0.2 convolution_convert_fusion.4
  26.9 0.6 broadcast_in_dim.32
  27.6 6.5 %all-to-all-start = ((bf16[2,16,1024]{2,1,0:T(8,128)(2,1)}), bf16[2,16,1024]{2,1,0:T(8,128)(2,1)S(1)}, u32[]{:S(2)}, u32[]{:S(2)}) async-start(bf16[2,16,1024]{2,1,0:T(8,128)(2,1)} %broadcast_in_dim.32), calls=%async_computation | async-start | bytes 131072 | tf_op jit(solution)/shard_map/all_to_all | solution.py:30
  34.0 1.1 all-to-all-done
  35.1 0.1 fusion.29
  35.3 0.1 fusion.31
  35.4 14.2 %all_to_all.35 = bf16[8,16,512]{2,1,0:T(8,128)(2,1)S(1)} all-to-all(bf16[8,16,512]{2,1,0:T(8,128)(2,1)S(1)} %broadcast_in_dim.33), channel_id=1, replica_groups=mesh['ep_0'=8,'ep_1'=4,'ep_2'=4,'tp'=2] {'ep_0'}, dimensions={0} | all-to-all | bytes 262144 | tf_op jit(solution)/shard_map/all_to_all | solution.py:30
  49.6 0.2 broadcast_in_dim.34
  49.9 33.8 %all_to_all.36 = bf16[16,8,16,512]{3,2,1,0:T(8,128)(2,1)S(1)} all-to-all(bf16[16,8,16,512]{3,2,1,0:T(8,128)(2,1)S(1)} %broadcast_in_dim.34), channel_id=1, replica_groups=mesh['ep_0'=8,'ep_1'=4,'ep_2'=4,'tp'=2] {'ep_1','ep_2'}, dimensions={0} | all-to-all | bytes 4194304 | tf_op jit(solution)/shard_map/all_to_all | solution.py:30
  83.7 0.2 copy.93
  83.9 0.7 convolution_convert_fusion
  84.7 0.7 convolution_convert_fusion.1
  85.5 6.9 %all_to_all.37 = bf16[2,2048,64]{1,2,0:T(8,128)(2,1)S(1)} all-to-all(bf16[2,2048,64]{1,2,0:T(8,128)(2,1)S(1)} %broadcast_in_dim.35), channel_id=1, replica_groups=mesh['ep_0'=8,'ep_1'=4,'ep_2'=4,'tp'=2] {'tp'}, dimensions={0} | all-to-all | bytes 1048576 | tf_op jit(solution)/shard_map/all_to_all | solution.py:30
  92.3 0.1 convert_reduce_fusion
  92.5 2.7 %fusion.25 = f32[2048,512]{1,0:T(8,128)} fusion(bf16[32,512]{1,0:T(8,128)(2,1)S(1)} %copy-done.6, f32[2048,64]{0,1:T(8,128)S(1)} %convert_reduce_fusion), kind=kOutput, calls=%fused_computation.42 | convolution fusion | flops 67502080 | bytes 4751360 | tf_op jit(solution)/shard_map/dot_general | solution.py:94
  95.1 0.0 reduce-scatter.4.cloned.1.call-update
  95.2 0.1 fusion.37
  95.3 0.4 fusion
  95.7 1.2 copy.94
  96.8 6.2 %all-to-all-start.4 = ((bf16[128,2,1024]{2,1,0:T(2,128)(2,1)}), bf16[128,2,1024]{2,1,0:T(2,128)(2,1)S(1)}, u32[]{:S(2)}, u32[]{:S(2)}) async-start(bf16[128,2,1024]{2,1,0:T(2,128)(2,1)} %copy.94), calls=%async_computation.7 | async-start | bytes 1048576 | tf_op jit(solution)/shard_map/all_to_all | solution.py:205
  103.0 0.0 reduce-scatter.6.cloned.1.call-start
  103.1 51.0 %reduce-scatter.4.cloned.1.call-done = f32[256,512]{1,0:T(8,128)} async-done(((f32[2048,512]{1,0:T(8,128)}), f32[256,512]{1,0:T(8,128)}) %reduce-scatter.4.cloned.1.call-update) | async-done | bytes 524304 | tf_op jit(solution)/shard_map/reduce_scatter | solution.py:54
  154.0 0.0 reduce-scatter.6.cloned.1.call-update
  154.1 0.2 reshape.241
  154.3 0.3 fusion.21
  154.6 0.3 fusion.4
  154.9 0.3 convolution_convert_fusion.2
  155.2 4.5 %all_to_all.38 = bf16[2,128,2,512]{3,1,2,0:T(8,128)(2,1)S(1)} all-to-all(bf16[2,128,2,512]{3,1,2,0:T(8,128)(2,1)S(1)} %bitcast.163), channel_id=1, replica_groups=mesh['ep_0'=8,'ep_1'=4,'ep_2'=4,'tp'=2] {'tp'}, dimensions={0} | all-to-all | bytes 1048576 | tf_op jit(solution)/shard_map/all_to_all | solution.py:24
  159.7 0.1 reduce_sum.85
  159.8 1.0 copy.97
  160.8 11.2 %all-to-all-start.6 = ((bf16[128,2,512]{2,1,0:T(2,128)(2,1)}), bf16[128,2,512]{2,1,0:T(2,128)(2,1)S(1)}, u32[]{:S(2)}, u32[]{:S(2)}) async-start(bf16[128,2,512]{2,1,0:T(2,128)(2,1)} %copy.97), calls=%async_computation.9 | async-start | bytes 524288 | tf_op jit(solution)/shard_map/all_to_all | solution.py:210
  172.0 0.0 reduce-scatter.8.cloned.1.call-start
  172.0 5.3 %reduce-scatter.6.cloned.1.call-done = f32[64,512]{1,0:T(8,128)} async-done(((f32[256,512]{1,0:T(8,128)}), f32[64,512]{1,0:T(8,128)}) %reduce-scatter.6.cloned.1.call-update) | async-done | bytes 131088 | tf_op jit(solution)/shard_map/reduce_scatter | solution.py:54
  177.4 0.1 select_reduce_fusion
  177.5 0.1 fusion.12
  177.6 8.1 %all-to-all-done.6 = bf16[128,2,512]{2,1,0:T(2,128)(2,1)S(1)} async-done(((bf16[128,2,512]{2,1,0:T(2,128)(2,1)}), bf16[128,2,512]{2,1,0:T(2,128)(2,1)S(1)}, u32[]{:S(2)}, u32[]{:S(2)}) %all-to-all-start.6) | async-done | bytes 262176 | tf_op jit(solution)/shard_map/all_to_all | solution.py:210
  185.7 18.7 %reduce-scatter.8.cloned.1.call-done = f32[16,512]{1,0:T(8,128)} async-done(((f32[64,512]{1,0:T(8,128)}), f32[16,512]{1,0:T(8,128)}) %reduce-scatter.8.cloned.1.call-update) | async-done | bytes 32784 | tf_op jit(solution)/shard_map/reduce_scatter | solution.py:54
  204.4 1.6 fusion.7
  (55 shorter events, 0.4 us)
Async XLA Ops:
  6.5 20.1 %copy-start = (bf16[512,1024]{1,0:T(8,128)(2,1)S(1)}, bf16[512,1024]{1,0:T(8,128)(2,1)}, u32[]{:S(2)}) copy-start(bf16[512,1024]{1,0:T(8,128)(2,1)} %param.28) | copy-start | bytes 3145732
  19.1 4.1 %copy-start.10 = (f32[4]{0:T(128)S(1)}, f32[4]{0:T(128)}, u32[]{:S(2)}) copy-start(f32[4]{0:T(128)} %param.26) | copy-start | bytes 52
  19.1 4.3 %copy-start.1 = (bf16[16,1024]{1,0:T(8,128)(2,1)S(1)}, bf16[16,1024]{1,0:T(8,128)(2,1)}, u32[]{:S(2)}) copy-start(bf16[16,1024]{1,0:T(8,128)(2,1)} %param.21) | copy-start | bytes 98308
  19.1 4.3 %copy-start.8 = (f32[1024]{0:T(1024)S(1)}, f32[1024]{0:T(1024)}, u32[]{:S(2)}) copy-start(f32[1024]{0:T(1024)} %param.22) | copy-start | bytes 12292
  19.1 4.3 %copy-start.13 = (bf16[1024,128]{1,0:T(8,128)(2,1)S(1)}, bf16[1024,128]{1,0:T(8,128)(2,1)}, u32[]{:S(2)}) copy-start(bf16[1024,128]{1,0:T(8,128)(2,1)} %param.25) | copy-start | bytes 786436
  22.1 4.4 %copy-start.12 = (f32[128]{0:T(128)S(1)}, f32[128]{0:T(128)}, u32[]{:S(2)}) copy-start(f32[128]{0:T(128)} %param.27) | copy-start | bytes 1540
  22.1 13.1 %copy-start.9 = (f32[1024]{0:T(1024)S(1)}, f32[1024]{0:T(1024)}, u32[]{:S(2)}) copy-start(f32[1024]{0:T(1024)} %param.32) | copy-start | bytes 12292
  27.6 7.6 %all-to-all-start = ((bf16[2,16,1024]{2,1,0:T(8,128)(2,1)}), bf16[2,16,1024]{2,1,0:T(8,128)(2,1)S(1)}, u32[]{:S(2)}, u32[]{:S(2)}) async-start(bf16[2,16,1024]{2,1,0:T(8,128)(2,1)} %broadcast_in_dim.32), calls=%async_computation | async-start | bytes 131072 | tf_op jit(solution)/shard_map/all_to_all | solution.py:30
  34.0 120.0 %reduce-scatter.4.cloned.1.call-start = ((), (), s32[]{:S(2)}) async-start(), calls=%async_computation.10 | async-start | bytes 4718592 | tf_op jit(solution)/shard_map/reduce_scatter | solution.py:54
  49.8 34.1 %copy-start.4 = (bf16[512,32]{0,1:T(8,128)(2,1)S(1)}, bf16[512,32]{0,1:T(8,128)(2,1)}, u32[]{:S(2)}) copy-start(bf16[512,32]{0,1:T(8,128)(2,1)} %param.39) | copy-start | bytes 98308
  83.7 1.0 copy-start.5
  83.9 8.5 %copy-start.6 = (bf16[32,512]{1,0:T(8,128)(2,1)S(1)}, bf16[32,512]{1,0:T(8,128)(2,1)}, u32[]{:S(2)}) copy-start(bf16[32,512]{1,0:T(8,128)(2,1)} %param.40) | copy-start | bytes 98308
  92.4 2.7 %copy-start.7 = (s32[16,6]{0,1:T(8,128)S(1)}, s32[16,6]{0,1:T(8,128)}, u32[]{:S(2)}) copy-start(s32[16,6]{0,1:T(8,128)} %param.33) | copy-start | bytes 1156
  95.1 59.1 %copy-start.2 = (bf16[1,1024,128]{2,1,0:T(8,128)(2,1)S(1)}, bf16[1,1024,128]{2,1,0:T(8,128)(2,1)}, u32[]{:S(2)}) copy-start(bf16[1,1024,128]{2,1,0:T(8,128)(2,1)} %param.35) | copy-start | bytes 786436
  95.1 59.4 %copy-start.14 = (bf16[1,1024,128]{2,1,0:T(8,128)(2,1)S(1)}, bf16[1,1024,128]{2,1,0:T(8,128)(2,1)}, u32[]{:S(2)}) copy-start(bf16[1,1024,128]{2,1,0:T(8,128)(2,1)} %param.36) | copy-start | bytes 786436
  95.2 59.7 %copy-start.3 = (bf16[1,128,1024]{2,1,0:T(8,128)(2,1)S(1)}, bf16[1,128,1024]{2,1,0:T(8,128)(2,1)}, u32[]{:S(2)}) copy-start(bf16[1,128,1024]{2,1,0:T(8,128)(2,1)} %param.37) | copy-start | bytes 786436
  96.8 57.2 %all-to-all-start.4 = ((bf16[128,2,1024]{2,1,0:T(2,128)(2,1)}), bf16[128,2,1024]{2,1,0:T(2,128)(2,1)S(1)}, u32[]{:S(2)}, u32[]{:S(2)}) async-start(bf16[128,2,1024]{2,1,0:T(2,128)(2,1)} %copy.94), calls=%async_computation.7 | async-start | bytes 1048576 | tf_op jit(solution)/shard_map/all_to_all | solution.py:205
  103.0 74.3 %reduce-scatter.6.cloned.1.call-start = ((), (), s32[]{:S(2)}) async-start(), calls=%async_computation.11 | async-start | bytes 655360 | tf_op jit(solution)/shard_map/reduce_scatter | solution.py:54
  154.0 18.0 %copy-start.11 = (bf16[16,6]{0,1:T(8,128)(2,1)S(1)}, bf16[16,6]{0,1:T(8,128)(2,1)}, u32[]{:S(2)}) copy-start(bf16[16,6]{0,1:T(8,128)(2,1)} %param.34) | copy-start | bytes 580
  154.0 23.4 %copy-start.15 = (f32[1024]{0:T(1024)S(1)}, f32[1024]{0:T(1024)}, u32[]{:S(2)}) copy-start(f32[1024]{0:T(1024)} %param.41) | copy-start | bytes 12292
  160.8 24.9 %all-to-all-start.6 = ((bf16[128,2,512]{2,1,0:T(2,128)(2,1)}), bf16[128,2,512]{2,1,0:T(2,128)(2,1)S(1)}, u32[]{:S(2)}, u32[]{:S(2)}) async-start(bf16[128,2,512]{2,1,0:T(2,128)(2,1)} %copy.97), calls=%async_computation.9 | async-start | bytes 524288 | tf_op jit(solution)/shard_map/all_to_all | solution.py:210
  172.0 32.4 %reduce-scatter.8.cloned.1.call-start = ((), (), s32[]{:S(2)}) async-start(), calls=%async_computation.12 | async-start | bytes 163840 | tf_op jit(solution)/shard_map/reduce_scatter | solution.py:54
Sparse Core Ops, SparseCore 0:
  95.3 58.6 reduce-scatter.3
  156.5 20.7 reduce-scatter.5
  179.8 24.5 reduce-scatter.7
where the time goes:
time: 215 us; the launch traced here: 213 us
  waiting for transfers between devices  84.2 us (39%)
  blocking collectives  59.4 us (28%)
  starting transfers between devices  23.9 us (11%)
  matrix products  16.5 us (8%)
  between operations  13.5 us (6%)
  local copies, waits for them, and re-layouts  10.9 us (5%)
  other arithmetic  4.17 us (2%)
    reduce_scatter x3, waiting for transfers between devices, scatter_axes(): shard = lax.psum_scatter(shard, axis, scatter_dimension=dim, tiled=True)  75 us
    all_to_all x3, blocking collectives, from_everyone(): lax.all_to_all(jnp.broadcast_to(shard[None], (devices, *shard.shape)), ax...  54.9 us
    all_to_all x1, starting transfers between devices, shards(): lax.all_to_all(expert_out, EP, split_axis=0, concat_axis=0, tiled=True)  11.2 us
    all_to_all x1, waiting for transfers between devices, shards(): lax.all_to_all(expert_out, EP, split_axis=0, concat_axis=0, tiled=True)  8.09 us
    unnamed x33, local copies, waits for them, and re-layouts  6.5 us
    all_to_all x1, starting transfers between devices, from_everyone(): lax.all_to_all(jnp.broadcast_to(shard[None], (devices, *shard.shape)), ax...  6.48 us
    all_to_all x1, starting transfers between devices, shards(): lax.all_to_all(outgoing, EP, split_axis=0, concat_axis=0, tiled=True)  6.16 us
    all_to_all x1, blocking collectives, sum_at_owner(): lax.all_to_all(split_up(shard, dim, devices), axis, 0, 0, tiled=True)  4.49 us
  transfers between devices with their start and end apart: 6, of which 5 were waited for; matrix products, arithmetic and copies ran while one was open for 2% of the time, Pallas kernels for 0%

commit v1 on v0

v1 whole, which is shorter than its diff:
```python
import math
import jax
import jax.numpy as jnp
from jax import lax
from jax.experimental import pallas as pl
from jax.experimental.pallas import tpu as pltpu
from jax.sharding import Mesh
from jax.sharding import PartitionSpec as P

HD = 64
NORM_EPS = 1e-06
HEAD_EPS = 1e-05
THETA = 500000.0
LAMBDA_BASE = 0.2
F32 = jnp.float32
BF16 = jnp.bfloat16
BLOCKS = 4


def attention_body(
    lens, lam, tokens, mixer_gain, wq_hbm, wk_hbm, wv_hbm, head_gain, wo_hbm, keys_hbm, values_hbm,
    out, wq, wk, wv, wo, keys, values, qrows, scores, mixed, wsem, ksem, vsem,
):
    seqs, span, width = keys.shape
    heads = lam.shape[0]
    rows = seqs * heads
    block = span // BLOCKS
    weights = [
        pltpu.make_async_copy(src, dst, wsem.at[i])
        for i, (src, dst) in enumerate(((wk_hbm, wk), (wq_hbm, wq), (wv_hbm, wv), (wo_hbm, wo)))
    ]
    key_copies = [
        pltpu.make_async_copy(
            keys_hbm.at[:, pl.ds(b * block, block), :], keys.at[:, pl.ds(b * block, block), :], ksem.at[b]
        )
        for b in range(BLOCKS)
    ]
    value_copies = [
        pltpu.make_async_copy(
            values_hbm.at[pl.ds(b * 4, 4)], values.at[pl.ds(b * 4, 4)], vsem.at[b]
        )
        for b in range(seqs // 4)
    ]
    for copy in weights[:3] + key_copies + value_copies + weights[3:]:
        copy.start()

    resid = tokens[...].astype(F32)
    mean_square = jnp.mean(resid * resid, axis=-1, keepdims=True)
    normed = (resid * lax.rsqrt(mean_square + NORM_EPS) * mixer_gain[...]).astype(BF16)

    row = lax.broadcasted_iota(jnp.int32, (seqs, width), 0)
    lane = lax.broadcasted_iota(jnp.int32, (seqs, width), 1)
    position = jnp.zeros((seqs, width), jnp.int32)
    for s in range(seqs):
        position = jnp.where(row == s, lens[s], position)
    half = HD // 2
    frequency = jnp.exp((lane % half).astype(F32) * (-2.0 / HD * math.log(THETA)))
    angles = position.astype(F32) * frequency
    first = lane % HD < half
    cos_vals = jnp.cos(angles)
    sin_vals = jnp.sin(angles)
    sin_vals = jnp.where(first, -sin_vals, sin_vals)

    def rotate(tile):
        swapped = jnp.where(first, pltpu.roll(tile, width - half, 1), pltpu.roll(tile, half, 1))
        return (tile * cos_vals + swapped * sin_vals).astype(BF16).astype(F32)

    column = lax.broadcasted_iota(jnp.int32, (1, width), 1)
    owner = column % rows // heads
    limit = jnp.zeros((1, width), jnp.int32)
    for s in range(seqs):
        limit = jnp.where(owner == s, lens[s], limit)
    mult = jnp.ones((1, width), F32)
    for j in range(heads):
        mult = jnp.where(column == rows + column % rows // heads * heads + j, lam[j], mult)

    weights[0].wait()
    knew = rotate(jnp.dot(normed, wk[...], preferred_element_type=F32)).astype(BF16)
    weights[1].wait()
    query_raw = jnp.dot(normed, wq[...], preferred_element_type=F32)
    for j in range(heads):
        tile = rotate(query_raw[:, j * width : (j + 1) * width]) * HD ** (-0.5)
        qrows[pl.ds(j, seqs, stride=heads), :] = jnp.where(lane < HD, tile, 0.0)
        qrows[pl.ds(rows + j, seqs, stride=heads), :] = jnp.where(lane < HD, 0.0, tile)
    qcols = jnp.transpose(qrows[...])
    query = jnp.concatenate([jnp.where(owner == s, qcols, 0.0).astype(BF16) for s in range(seqs)], axis=0)
    weights[2].wait()
    vnew = jnp.dot(normed, wv[...], preferred_element_type=F32).astype(BF16).astype(F32)
    for j in range(heads):
        mixed[pl.ds(j, seqs, stride=heads), :] = vnew

    new_row = jnp.concatenate([knew[s : s + 1, :] for s in range(seqs)], axis=1)
    new_row = jnp.broadcast_to(new_row, (16, seqs * width))
    new_score = jnp.dot(new_row, query, preferred_element_type=F32)[:1]
    peak = new_score
    for b in range(BLOCKS):
        key_copies[b].wait()
        past = jnp.concatenate([keys[s, pl.ds(b * block, block), :] for s in range(seqs)], axis=1)
        score = jnp.dot(past, query, preferred_element_type=F32)
        place = lax.broadcasted_iota(jnp.int32, (block, width), 0) + b * block
        score = jnp.where(place < limit, score, -jnp.inf)
        scores[pl.ds(b * block, block), :] = score
        peak = jnp.maximum(peak, jnp.max(score, axis=0, keepdims=True))
    expo = jnp.exp(scores[...] - peak)
    expo_new = jnp.exp(new_score - peak)
    factor = mult / (jnp.sum(expo, axis=0, keepdims=True) + expo_new)
    scaled = expo * factor
    weight = jnp.transpose(scaled - pltpu.roll(scaled, rows, 1))[:rows].astype(BF16)
    scaled_new = jnp.broadcast_to(expo_new * factor, (width, width))
    weight_new = jnp.transpose(scaled_new - pltpu.roll(scaled_new, rows, 1))[:rows].astype(BF16).astype(F32)
    pair = 8 // heads
    part = lax.broadcasted_iota(jnp.int32, (8, width), 0) // heads
    for g in range(seqs // pair):
        group = jnp.zeros((8, width), F32)
        for i in range(pair):
            s = g * pair + i
            if s % 4 == 0:
                value_copies[s // 4].wait()
            own = jnp.dot(weight[g * 8 : g * 8 + 8], values[s], preferred_element_type=F32)
            group = jnp.where(part == i, own, group)
        where = pl.ds(g * 8, 8)
        mixed[where, :] = group + weight_new[g * 8 : g * 8 + 8] * mixed[where, :]
    mix = mixed[...]
    mix_square = jnp.mean(mix * mix, axis=-1, keepdims=True)
    mixed[...] = mix * lax.rsqrt(mix_square + HEAD_EPS) * head_gain[...] * (1.0 - LAMBDA_BASE)
    head_out = jnp.concatenate([mixed[pl.ds(j, seqs, stride=heads), :] for j in range(heads)], axis=1)
    weights[3].wait()
    out[...] = jnp.dot(head_out.astype(BF16), wo[...], preferred_element_type=F32)


def attention(lens, lam, tokens, mixer_gain, wq, wk, wv, head_gain, wo, cache_keys, cache_values):
    seqs, model_width = tokens.shape
    span, width = cache_keys.shape[1:]
    heads = lam.shape[0]
    smem = pl.BlockSpec(memory_space=pltpu.SMEM)
    vmem = pl.BlockSpec(memory_space=pltpu.VMEM)
    hbm = pl.BlockSpec(memory_space=pltpu.HBM)
    return pl.pallas_call(
        attention_body,
        out_shape=jax.ShapeDtypeStruct((seqs, model_width), F32),
        in_specs=[smem, smem, vmem, vmem, hbm, hbm, hbm, vmem, hbm, hbm, hbm],
        out_specs=vmem,
        scratch_shapes=[
            pltpu.VMEM(wq.shape, BF16),
            pltpu.VMEM(wk.shape, BF16),
            pltpu.VMEM(wv.shape, BF16),
            pltpu.VMEM(wo.shape, BF16),
            pltpu.VMEM((seqs, span, width), BF16),
            pltpu.VMEM((seqs, span, width), BF16),
            pltpu.VMEM((2 * seqs * heads, width), F32),
            pltpu.VMEM((span, width), F32),
            pltpu.VMEM((seqs * heads, width), F32),
            pltpu.SemaphoreType.DMA((4,)),
            pltpu.SemaphoreType.DMA((BLOCKS,)),
            pltpu.SemaphoreType.DMA((4,)),
        ],
        compiler_params=pltpu.CompilerParams(vmem_limit_bytes=62 * 1024 * 1024),
        cost_estimate=pl.CostEstimate(flops=10**9, bytes_accessed=12 * 1024 * 1024, transcendentals=10**6),
        name="attention",
    )(lens, lam, tokens, mixer_gain, wq, wk, wv, head_gain, wo, cache_keys, cache_values)


EP = ("zh", "zl", "yh", "yl", "xh", "xl")
SMEM = pl.BlockSpec(memory_space=pltpu.SMEM)
VMEM = pl.BlockSpec(memory_space=pltpu.VMEM)


def call(body, name, out_shape, in_specs, scratch=(), flops=10**8):
    return pl.pallas_call(
        body,
        out_shape=out_shape,
        in_specs=in_specs,
        out_specs=jax.tree.map(lambda _: VMEM, out_shape),
        scratch_shapes=list(scratch),
        compiler_params=pltpu.CompilerParams(vmem_limit_bytes=24 * 1024 * 1024),
        cost_estimate=pl.CostEstimate(flops=flops, bytes_accessed=2 * 1024 * 1024, transcendentals=10**5),
        name=name,
    )


def pack_body(gate, up, down, out):
    units = down.shape[0]
    out[pl.ds(0, units), :] = jnp.transpose(gate[...].astype(F32)).astype(BF16)
    out[pl.ds(units, units), :] = jnp.transpose(up[...].astype(F32)).astype(BF16)
    out[pl.ds(2 * units, units), :] = down[...]


def mid_body(core, tokens, own, other, channel_gain, ids, shares, branch_gate, send, mid, pick, gate, slab):
    seqs, model_width = tokens.shape
    peers, lines, width = send.shape
    chunks = model_width // width
    summed = (tokens[...].astype(F32) + (own[...] + other[...])).astype(BF16)
    mid[...] = summed
    wide = summed.astype(F32)
    mean_square = jnp.mean(wide * wide, axis=-1, keepdims=True)
    ffn = (wide * lax.rsqrt(mean_square + NORM_EPS) * channel_gain[...]).astype(BF16)
    logit = jnp.sum(ffn.astype(F32) * branch_gate[...], axis=-1, keepdims=True)
    gate[...] = jnp.broadcast_to(jax.nn.sigmoid(logit), gate.shape)

    peer = lax.broadcasted_iota(jnp.int32, (seqs, peers), 1)
    row = lax.broadcasted_iota(jnp.int32, (seqs, peers), 0)
    share = jnp.zeros((seqs, peers), F32)
    picked = jnp.zeros((seqs, peers), F32)
    for k in range(ids.shape[1]):
        named = ids[:, k : k + 1] == peer
        picked = jnp.where(named, 1.0, picked)
        share = jnp.where(named, shares[:, k : k + 1].astype(F32), share)
    above = lax.broadcasted_iota(jnp.int32, (seqs, seqs), 0) >= lax.broadcasted_iota(jnp.int32, (seqs, seqs), 1)
    rank = jnp.dot(above.astype(BF16), picked.astype(BF16), preferred_element_type=F32)
    placed = (picked > 0.0) & (rank == (core[0] + 1).astype(F32))
    pick[...] = jnp.where(placed, share, 0.0).astype(BF16)
    dense = row == 2 * member(peer) + core[0]
    for r, chosen in enumerate((placed, dense)):
        lines_out = lax.dot_general(
            chosen.astype(F32).astype(BF16), ffn, (((0,), (0,)), ((), ())), preferred_element_type=F32
        )
        for k in range(chunks):
            slab[pl.ds(r * chunks + k, peers, stride=lines), :] = lines_out[:, k * width : (k + 1) * width]
    send[...] = slab[...].reshape(send.shape).astype(BF16)


def member(peer):
    return (peer // 16 % 2) * 4 + (peer // 4 % 2) * 2 + peer % 2


def unpack(slab, first, chunks, lines):
    peers = slab.shape[0] // lines
    return [slab[pl.ds(first + k, peers, stride=lines), :].astype(BF16) for k in range(chunks)]


def experts_body(
    core, arrived, gate_own, gate_other, up_own, up_other, down_own, down_other, dense_own, dense_other, out, slab
):
    peers, lines, width = arrived.shape
    chunks = lines // 2
    slab[...] = arrived[...].reshape(slab.shape).astype(F32)
    routed = jnp.concatenate(unpack(slab, 0, chunks, lines), axis=1)
    tokens = unpack(slab, chunks, chunks, lines)
    low, high = jnp.concatenate(tokens[: chunks // 2], axis=1), jnp.concatenate(tokens[chunks // 2 :], axis=1)
    is_first = core[0] == 0
    result = jnp.zeros((peers, chunks * width), F32)
    for w_gate, w_up, w_down in ((gate_own, up_own, down_own), (gate_other, up_other, down_other)):
        gate_part = jnp.dot(routed, w_gate[0], preferred_element_type=F32)
        up_part = jnp.dot(routed, w_up[0], preferred_element_type=F32)
        hidden = (jax.nn.silu(gate_part) * up_part).astype(BF16)
        result = result + jnp.dot(hidden, w_down[0], preferred_element_type=F32)
    for k in range(chunks):
        slab[pl.ds(k, peers, stride=lines), :] = result[:, k * width : (k + 1) * width]

    blocks, stacked, half_width = dense_own.shape
    units = stacked // 3

    def part(ref, i):
        return ref[:, i * units : (i + 1) * units, :].reshape(blocks * units, half_width)

    mine, theirs = jnp.where(is_first, low, high), jnp.where(is_first, high, low)

    def project(i):
        dims = (((1,), (1,)), ((), ()))
        return lax.dot_general(mine, part(dense_own, i), dims, preferred_element_type=F32) + lax.dot_general(
            theirs, part(dense_other, i), dims, preferred_element_type=F32
        )

    hidden = (jax.nn.silu(project(0)) * project(1)).astype(BF16)
    sum_own = jnp.dot(hidden, part(dense_own, 2), preferred_element_type=F32)
    sum_other = jnp.dot(hidden, part(dense_other, 2), preferred_element_type=F32)
    halves = (jnp.where(is_first, sum_own, sum_other), jnp.where(is_first, sum_other, sum_own))
    for h, value in enumerate(halves):
        for k in range(chunks // 2):
            where = pl.ds(chunks + h * chunks // 2 + k, peers, stride=lines)
            slab[where, :] = value[:, k * width : (k + 1) * width]
    out[...] = slab[...].reshape(out.shape).astype(BF16)


def combine_body(core, returned, pick, gate, mid, keep, send, slab):
    peers, lines, width = returned.shape
    chunks = lines // 2
    seqs = pick.shape[0]
    slab[...] = returned[...].reshape(slab.shape).astype(F32)
    peer = lax.broadcasted_iota(jnp.int32, (seqs, peers), 1)
    row = lax.broadcasted_iota(jnp.int32, (seqs, peers), 0)
    dense = (row == 2 * member(peer) + core[0]).astype(F32).astype(BF16)
    routed = jnp.dot(pick[...], jnp.concatenate(unpack(slab, 0, chunks, lines), axis=1), preferred_element_type=F32)
    branch = jnp.dot(dense, jnp.concatenate(unpack(slab, chunks, chunks, lines), axis=1), preferred_element_type=F32)
    total = routed + gate[:, :1] * branch
    half = chunks * width // 2
    is_first = core[0] == 0
    low, high = total[:, :half], total[:, half:]
    resid = mid[...].astype(F32)
    keep[...] = jnp.where(is_first, resid[:, :half] + low, resid[:, half:] + high)
    send[...] = jnp.where(is_first, high, low)


def swap(value, axis):
    return lax.ppermute(value, axis, [(0, 1), (1, 0)])


def shards(
    tokens, mixer_gain, query_weight, key_weight, value_weight, head_lambda, head_gain, out_weight,
    cache_keys, cache_values, seq_lengths, channel_gain, expert_ids, expert_shares,
    expert_gate, expert_up, expert_down, dense_gate, dense_up, dense_down, branch_gate,
):
    seqs, model_width = tokens.shape
    peers = lax.axis_size(EP)
    width = 2 * HD
    lines = 2 * model_width // width
    half = model_width // 2
    core = lax.axis_index("tp").astype(jnp.int32).reshape(1)
    sds = jax.ShapeDtypeStruct
    slab = pltpu.VMEM((peers * lines, width), F32)

    gate_other, up_other, down_other = (swap(w, "tp") for w in (expert_gate, expert_up, expert_down))
    units = dense_down.shape[0]
    packed = call(pack_body, "pack", sds((3 * units, half), BF16), [VMEM] * 3)(dense_gate, dense_up, dense_down)
    gathered = packed[None]
    for axis in ("xl", "yl", "zl"):
        gathered = jnp.concatenate([gathered, swap(gathered, axis)], axis=0)
    gathered_other = swap(gathered, "tp")

    own = attention(
        seq_lengths, head_lambda, tokens, mixer_gain.reshape(1, -1), query_weight, key_weight, value_weight,
        head_gain.reshape(1, -1), out_weight, cache_keys, cache_values,
    )
    other = swap(own, "tp")
    send, mid, pick, gate = call(
        mid_body,
        "mid",
        (
            sds((peers, lines, width), BF16),
            sds((seqs, model_width), BF16),
            sds((seqs, peers), BF16),
            sds((seqs, width), F32),
        ),
        [SMEM] + [VMEM] * 7,
        [slab],
    )(core, tokens, own, other, channel_gain.reshape(1, -1), expert_ids, expert_shares, branch_gate.reshape(1, -1))
    arrived = lax.all_to_all(send, EP, 0, 0, tiled=True)
    rows_out = call(experts_body, "experts", sds((peers, lines, width), BF16), [SMEM] + [VMEM] * 9, [slab])(
        core, arrived, expert_gate, gate_other, expert_up, up_other, expert_down, down_other, gathered, gathered_other
    )
    returned = lax.all_to_all(rows_out, EP, 0, 0, tiled=True)
    keep, give = call(
        combine_body, "combine", (sds((seqs, half), F32), sds((seqs, half), F32)), [SMEM] + [VMEM] * 4, [slab]
    )(core, returned, pick, gate, mid)
    return (keep + swap(give, "tp")).astype(BF16)


def solution(mesh):
    torus = Mesh(mesh.devices.reshape(4, 2, 2, 2, 2, 2, 2), (*EP, "tp"))
    return jax.shard_map(
        shards,
        mesh=torus,
        in_specs=(
            P(EP, None),
            P(),
            P(None, "tp"),
            P(None, "tp"),
            P(None, "tp"),
            P("tp"),
            P(),
            P("tp", None),
            P(EP, None, "tp"),
            P(EP, None, "tp"),
            P(EP),
            P(),
            P(EP, None),
            P(EP, None),
            P(EP, None, "tp"),
            P(EP, None, "tp"),
            P(EP, "tp", None),
            P("tp", EP),
            P("tp", EP),
            P(EP, "tp"),
            P(),
        ),
        out_specs=P(EP, "tp"),
        check_vma=False,
    )
```

time: 215 us -> 94.9 us (0.44)
  waiting for transfers between devices: 84.2 us -> 22.6 us
  blocking collectives: 59.4 us -> 24.4 us
  matrix products: 16.5 us -> 0 us
  between operations: 13.5 us -> 0.12 us
  Pallas kernels: 0 us -> 11.5 us
  local copies, waits for them, and re-layouts: 10.9 us -> 5.22 us
  starting transfers between devices: 23.9 us -> 28.9 us
  other arithmetic: 4.17 us -> 1.75 us
    reduce_scatter x3 -> x0, waiting for transfers between devices: 75 us -> none  [scatter_axes(): shard = lax.psum_scatter(shard, axis, scatter_dimension=dim, tiled=True)]
    all_to_all x4 -> x1, blocking collectives: 59.4 us -> 24.4 us  [shards(): returned = lax.all_to_all(rows_out, EP, 0, 0, tiled=True)]
    dot_general x16 -> x0, matrix products: 16.5 us -> none  [the longest x1 3.04 us: shards(): jnp.einsum('sgjcd,slgcd->sgjcl', query, key_rows, preferred_element_type=...]
    ppermute x0 -> x9, starting transfers between devices: none -> 14.3 us  [swap(): return lax.ppermute(value, axis, [(0, 1), (1, 0)])]
    pallas_call x0 -> x5, Pallas kernels: none -> 11.5 us  [the longest x1 7.76 us: attention(): pl.pallas_call(attention_body, out_shape=jax.ShapeDtypeStruct((seqs, mode...]
    ppermute x0 -> x9, waiting for transfers between devices: none -> 9.27 us  [swap(): return lax.ppermute(value, axis, [(0, 1), (1, 0)])]
    all_to_all x3 -> x1, starting transfers between devices: 23.8 us -> 14.6 us  [shards(): arrived = lax.all_to_all(send, EP, 0, 0, tiled=True)]
    all_to_all x3 -> x1, waiting for transfers between devices: 9.16 us -> 13.3 us  [shards(): arrived = lax.all_to_all(send, EP, 0, 0, tiled=True)]
  transfers between devices with their start and end apart: 6 -> 10, of which waited for: 5 -> 8; matrix products, arithmetic and copies ran while one was open for 2% -> 1% of each run, Pallas kernels for 0% -> 10%
where the time goes in v1:
time: 94.9 us; the launch traced here: 94.4 us
  starting transfers between devices  28.9 us (30%)
  blocking collectives  24.4 us (26%)
  waiting for transfers between devices  22.6 us (24%)
  Pallas kernels  11.5 us (12%)
  local copies, waits for them, and re-layouts  5.22 us (6%)
  other arithmetic  1.75 us (2%)
    all_to_all x1, blocking collectives, shards(): returned = lax.all_to_all(rows_out, EP, 0, 0, tiled=True)  24.4 us
    all_to_all x1, starting transfers between devices, shards(): arrived = lax.all_to_all(send, EP, 0, 0, tiled=True)  14.6 us
    ppermute x9, starting transfers between devices, swap(): return lax.ppermute(value, axis, [(0, 1), (1, 0)])  14.3 us
    all_to_all x1, waiting for transfers between devices, shards(): arrived = lax.all_to_all(send, EP, 0, 0, tiled=True)  13.3 us
    ppermute x9, waiting for transfers between devices, swap(): return lax.ppermute(value, axis, [(0, 1), (1, 0)])  9.27 us
    pallas_call x1, Pallas kernels, attention(): pl.pallas_call(attention_body, out_shape=jax.ShapeDtypeStruct((seqs, mode...  7.76 us
    unnamed x28, local copies, waits for them, and re-layouts  5.22 us
  transfers between devices with their start and end apart: 10, of which 8 were waited for; matrix products, arithmetic and copies ran while one was open for 1% of the time, Pallas kernels for 10%

profile of v1, /device:TPU:1, one launch (start us, length us, event | category | flops | bytes accessed | tf_op | source)
XLA Modules:
  0.0 94.4 jit_solution(16612204001346102602)
XLA Ops:
  0.0 0.9 copy.24.gate
  0.9 0.9 copy.25.up
  1.8 0.0 copy-start.7
  1.8 0.8 copy-done.7
  2.5 0.1 pack.1
  2.6 2.1 %collective-permute-start.4 = (bf16[1,96,512]{2,1,0:T(8,128)(2,1)S(1)}, bf16[1,96,512]{2,1,0:T(8,128)(2,1)S(1)}, u32[]{:S(2)}, u32[]{:S(2)}) collective-permute-start(bf16[1,96,512]{2,1,0:T(8,128)(2,1)S(1)} %bitcast.6), channel_id=1, source_target_pairs={{0,2},{2,0},{1,3},{3,1},{4,6},{6,4},{5,7},{7,5},{8,10},{10,8},{9,1... | collective-permute-start | bytes 294920 | tf_op jit(solution)/shard_map/ppermute | solution.py:295
  4.8 2.0 %collective-permute-done.4 = bf16[1,96,512]{2,1,0:T(8,128)(2,1)S(1)} collective-permute-done((bf16[1,96,512]{2,1,0:T(8,128)(2,1)S(1)}, bf16[1,96,512]{2,1,0:T(8,128)(2,1)S(1)}, u32[]{:S(2)}, u32[]{:S(2)}) %collective-permute-start.4) | collective-permute-done | bytes 98336 | tf_op jit(solution)/shard_map/ppermute | solution.py:295
  6.8 1.6 %collective-permute-start.5 = (bf16[2,96,512]{2,1,0:T(8,128)(2,1)S(1)}, bf16[2,96,512]{2,1,0:T(8,128)(2,1)S(1)}, u32[]{:S(2)}, u32[]{:S(2)}) collective-permute-start(bf16[2,96,512]{2,1,0:T(8,128)(2,1)S(1)} %pad_maximum_fusion.2), channel_id=1, source_target_pairs={{0,8},{8,0},{1,9},{9,1},{2,10},{10,2},{3,11},{11,3},{4,12},{12,4},... | collective-permute-start | bytes 589832 | tf_op jit(solution)/shard_map/ppermute | solution.py:295
  8.4 3.1 %collective-permute-done.5 = bf16[2,96,512]{2,1,0:T(8,128)(2,1)S(1)} collective-permute-done((bf16[2,96,512]{2,1,0:T(8,128)(2,1)S(1)}, bf16[2,96,512]{2,1,0:T(8,128)(2,1)S(1)}, u32[]{:S(2)}, u32[]{:S(2)}) %collective-permute-start.5) | collective-permute-done | bytes 196640 | tf_op jit(solution)/shard_map/ppermute | solution.py:295
  11.5 1.9 %collective-permute-start.6 = (bf16[4,96,512]{2,1,0:T(8,128)(2,1)S(1)}, bf16[4,96,512]{2,1,0:T(8,128)(2,1)}, u32[]{:S(2)}, u32[]{:S(2)}) collective-permute-start(bf16[4,96,512]{2,1,0:T(8,128)(2,1)S(1)} %pad_maximum_fusion.1), channel_id=1, source_target_pairs={{0,32},{32,0},{1,33},{33,1},{2,34},{34,2},{3,35},{35,3},{4,36},{36... | collective-permute-start | bytes 1179656 | tf_op jit(solution)/shard_map/ppermute | solution.py:295
  13.4 0.0 copy-start.11
  13.4 0.0 copy-start.10
  13.4 0.0 copy-start.6
  13.4 0.0 copy-start.8
  13.4 0.0 copy-start.9
  13.4 0.0 copy-start
  13.4 0.0 copy-start.1
  13.5 0.0 copy-start.2
  13.5 7.8 %attention.1.own = f32[16,1024]{1,0:T(8,128)} custom-call(s32[16]{0:T(128)} %lens.1, f32[4]{0:T(128)} %lam.1, bf16[16,1024]{1,0:T(8,128)(2,1)} %tokens.3, f32[1,1024]{1,0:T(1,128)} %bitcast.12, bf16[1024,512]{1,0:T(8,128)(2,1)} %wq_hbm.1, bf16[1024,128]{1,0:T(8,128)(2,1)} %wk_hbm.1, bf16[1024,128]{1,0:T(8,128)(2,1)} %wv_hbm.1, f32[1,128]{1,0:T(1,128)} %bitcast.13, ...), custom_call_target="tpu_custom_call" | custom-call | flops 1000000000 | bytes 12582912 | tf_op jit(solution)/shard_map/attention/pallas_call | solution.py:138
  21.2 3.3 %collective-permute-start = (f32[16,1024]{1,0:T(8,128)}, f32[16,1024]{1,0:T(8,128)S(1)}, u32[]{:S(2)}, u32[]{:S(2)}) collective-permute-start(f32[16,1024]{1,0:T(8,128)} %attention.1.own), channel_id=1, source_target_pairs={{0,1},{1,0},{2,3},{3,2},{4,5},{5,4},{6,7},{7,6},{8,9},{9,8},{10,11... | collective-permute-start | bytes 196616 | tf_op jit(solution)/shard_map/ppermute | solution.py:295
  24.6 0.0 copy-done.11
  24.6 0.1 copy.23.shares
  24.7 0.0 copy-done.10
  24.7 0.1 copy.22.ids
  24.8 0.9 collective-permute-done.other
  25.7 0.0 copy-done.6
  25.7 0.0 copy-done.8
  25.7 0.0 copy-done.9
  25.7 0.0 copy-start.5
  25.7 0.8 copy-done.5
  26.5 1.6 %mid.1 = (bf16[128,16,128]{2,1,0:T(8,128)(2,1)}, bf16[16,1024]{1,0:T(8,128)(2,1)S(1)}, bf16[16,128]{1,0:T(8,128)(2,1)S(1)}, f32[16,128]{1,0:T(8,128)S(1)}) custom-call(s32[1]{0:T(128)} %bitcast.core, bf16[16,1024]{1,0:T(8,128)(2,1)S(1)} %copy-done.6, f32[16,1024]{1,0:T(8,128)S(1)} %copy-done.5, f32[16,1024]{1,0:T(8,128)S(1)} %collective-permute-done.other, ...), custom_call_target="tpu_custom_call" | custom-call | flops 100000000 | bytes 2097152 | tf_op jit(solution)/shard_map/mid/pallas_call | solution.py:325
  28.1 14.6 %all-to-all-start = ((bf16[128,16,128]{2,1,0:T(8,128)(2,1)}), bf16[128,16,128]{2,1,0:T(8,128)(2,1)S(1)}, u32[]{:S(2)}, u32[]{:S(2)}) async-start(bf16[128,16,128]{2,1,0:T(8,128)(2,1)} %get-tuple-element.11), calls=%async_computation | async-start | bytes 1048576 | tf_op jit(solution)/shard_map/all_to_all | solution.py:337
  42.7 0.0 collective-permute-done.6
  42.7 1.1 %pad_maximum_fusion.dense_own = bf16[8,96,512]{2,1,0:T(8,128)(2,1)S(1)} fusion(bf16[4,96,512]{2,1,0:T(8,128)(2,1)} %collective-permute-done.6, bf16[2,96,512]{2,1,0:T(8,128)(2,1)S(1)} %collective-permute-done.5, bf16[1,96,512]{2,1,0:T(8,128)(2,1)S(1)} %collective-permute-done.4, bf16[1,96,512]{2,1,0:T(8,128)(2,1)S(1)} %bitcast.9), kind=kLoop, calls=%fused_computation | loop fusion | flops 1179648 | bytes 1572864 | tf_op jit(solution)/shard_map/concatenate | solution.py:317
  43.8 0.7 collective-permute-start.7
  44.5 0.0 copy-done
  44.5 0.1 collective-permute-start.1
  44.6 0.0 copy-done.1
  44.7 0.4 collective-permute-start.2
  45.1 0.0 copy-done.2
  45.1 0.1 collective-permute-start.3
  45.2 1.7 %collective-permute-done.1.gate_other = bf16[1,1024,128]{2,1,0:T(8,128)(2,1)S(1)} collective-permute-done((bf16[1,1024,128]{2,1,0:T(8,128)(2,1)S(1)}, bf16[1,1024,128]{2,1,0:T(8,128)(2,1)S(1)}, u32[]{:S(2)}, u32[]{:S(2)}) %collective-permute-start.1) | collective-permute-done | bytes 262176 | tf_op jit(solution)/shard_map/ppermute | solution.py:295
  46.8 0.4 collective-permute-done.2.up_other
  47.2 0.4 collective-permute-done.3.down_other
  47.6 0.0 copy-start.3
  47.6 0.7 copy-done.3
  48.3 13.3 %all-to-all-done.arrived = bf16[128,16,128]{2,1,0:T(8,128)(2,1)S(1)} async-done(((bf16[128,16,128]{2,1,0:T(8,128)(2,1)}), bf16[128,16,128]{2,1,0:T(8,128)(2,1)S(1)}, u32[]{:S(2)}, u32[]{:S(2)}) %all-to-all-start) | async-done | bytes 524320 | tf_op jit(solution)/shard_map/all_to_all | solution.py:337
  61.6 0.0 collective-permute-done.7.dense_other
  61.6 0.0 copy-start.4
  61.6 0.9 %copy-done.4 = bf16[1,128,1024]{2,1,0:T(8,128)(2,1)S(1)} copy-done((bf16[1,128,1024]{2,1,0:T(8,128)(2,1)S(1)}, bf16[1,128,1024]{2,1,0:T(8,128)(2,1)}, u32[]{:S(2)}) %copy-start.4) | copy-done | bytes 262168
  62.5 1.6 %experts.1 = bf16[128,16,128]{2,1,0:T(8,128)(2,1)S(1)} custom-call(s32[1]{0:T(128)} %bitcast.core, bf16[128,16,128]{2,1,0:T(8,128)(2,1)S(1)} %all-to-all-done.arrived, bf16[1,1024,128]{2,1,0:T(8,128)(2,1)S(1)} %copy-done, bf16[1,1024,128]{2,1,0:T(8,128)(2,1)S(1)} %collective-permute-done.1.gate_other, bf16[1,1024,128]{2,1,0:T(8,128)(2,1)S(1)} %copy-done.1, ...), custom_call_target="tpu_custom_call" | custom-call | flops 100000000 | bytes 2097152 | tf_op jit(solution)/shard_map/experts/pallas_call | solution.py:338
  64.1 24.4 %all_to_all.10.returned = bf16[128,16,128]{2,1,0:T(8,128)(2,1)S(1)} all-to-all(bf16[128,16,128]{2,1,0:T(8,128)(2,1)S(1)} %experts.1), channel_id=1, replica_groups=mesh['zh'=4,'zl'=2,'yh'=2,'yl'=2,'xh'=2,'xl'=2,'tp'=2] {'zh','zl','yh','..., dimensions={0} | all-to-all | bytes 1048576 | tf_op jit(solution)/shard_map/all_to_all | solution.py:341
  88.5 0.5 combine.1
  88.9 4.0 %collective-permute-start.8 = (f32[16,512]{1,0:T(8,128)S(1)}, f32[16,512]{1,0:T(8,128)S(1)}, u32[]{:S(2)}, u32[]{:S(2)}) collective-permute-start(f32[16,512]{1,0:T(8,128)S(1)} %get-tuple-element.16), channel_id=1, source_target_pairs={{0,1},{1,0},{2,3},{3,2},{4,5},{5,4},{6,7},{7,6},{8,9},{9,8},{10,11... | collective-permute-start | bytes 98312 | tf_op jit(solution)/shard_map/ppermute | solution.py:295
  92.9 0.9 collective-permute-done.8
  93.8 0.6 add_convert_fusion
  (2 shorter events, 0.1 us)
Async XLA Ops:
  1.8 0.8 copy-start.7
  2.6 4.1 %collective-permute-start.4 = (bf16[1,96,512]{2,1,0:T(8,128)(2,1)S(1)}, bf16[1,96,512]{2,1,0:T(8,128)(2,1)S(1)}, u32[]{:S(2)}, u32[]{:S(2)}) collective-permute-start(bf16[1,96,512]{2,1,0:T(8,128)(2,1)S(1)} %bitcast.6), channel_id=1, source_target_pairs={{0,2},{2,0},{1,3},{3,1},{4,6},{6,4},{5,7},{7,5},{8,10},{10,8},{9,1... | collective-permute-start | bytes 294920 | tf_op jit(solution)/shard_map/ppermute | solution.py:295
  6.8 4.7 %collective-permute-start.5 = (bf16[2,96,512]{2,1,0:T(8,128)(2,1)S(1)}, bf16[2,96,512]{2,1,0:T(8,128)(2,1)S(1)}, u32[]{:S(2)}, u32[]{:S(2)}) collective-permute-start(bf16[2,96,512]{2,1,0:T(8,128)(2,1)S(1)} %pad_maximum_fusion.2), channel_id=1, source_target_pairs={{0,8},{8,0},{1,9},{9,1},{2,10},{10,2},{3,11},{11,3},{4,12},{12,4},... | collective-permute-start | bytes 589832 | tf_op jit(solution)/shard_map/ppermute | solution.py:295
  11.5 31.2 %collective-permute-start.6 = (bf16[4,96,512]{2,1,0:T(8,128)(2,1)S(1)}, bf16[4,96,512]{2,1,0:T(8,128)(2,1)}, u32[]{:S(2)}, u32[]{:S(2)}) collective-permute-start(bf16[4,96,512]{2,1,0:T(8,128)(2,1)S(1)} %pad_maximum_fusion.1), channel_id=1, source_target_pairs={{0,32},{32,0},{1,33},{33,1},{2,34},{34,2},{3,35},{35,3},{4,36},{36... | collective-permute-start | bytes 1179656 | tf_op jit(solution)/shard_map/ppermute | solution.py:295
  13.4 11.2 %copy-start.11 = (bf16[16,6]{0,1:T(8,128)(2,1)S(1)}, bf16[16,6]{0,1:T(8,128)(2,1)}, u32[]{:S(2)}) copy-start(bf16[16,6]{0,1:T(8,128)(2,1)} %param.34) | copy-start | bytes 580
  13.4 11.3 %copy-start.10 = (s32[16,6]{0,1:T(8,128)S(1)}, s32[16,6]{0,1:T(8,128)}, u32[]{:S(2)}) copy-start(s32[16,6]{0,1:T(8,128)} %param.33) | copy-start | bytes 1156
  13.4 12.3 %copy-start.6 = (bf16[16,1024]{1,0:T(8,128)(2,1)S(1)}, bf16[16,1024]{1,0:T(8,128)(2,1)}, u32[]{:S(2)}) copy-start(bf16[16,1024]{1,0:T(8,128)(2,1)} %tokens.3) | copy-start | bytes 98308
  13.4 12.3 %copy-start.8 = (f32[1024]{0:T(1024)S(1)}, f32[1024]{0:T(1024)}, u32[]{:S(2)}) copy-start(f32[1024]{0:T(1024)} %param.32) | copy-start | bytes 12292
  13.4 12.3 %copy-start.9 = (f32[1024]{0:T(1024)S(1)}, f32[1024]{0:T(1024)}, u32[]{:S(2)}) copy-start(f32[1024]{0:T(1024)} %param.41) | copy-start | bytes 12292
  13.4 31.1 %copy-start = (bf16[1,1024,128]{2,1,0:T(8,128)(2,1)S(1)}, bf16[1,1024,128]{2,1,0:T(8,128)(2,1)}, u32[]{:S(2)}) copy-start(bf16[1,1024,128]{2,1,0:T(8,128)(2,1)} %gate_own.1) | copy-start | bytes 786436
  13.4 31.2 %copy-start.1 = (bf16[1,1024,128]{2,1,0:T(8,128)(2,1)S(1)}, bf16[1,1024,128]{2,1,0:T(8,128)(2,1)}, u32[]{:S(2)}) copy-start(bf16[1,1024,128]{2,1,0:T(8,128)(2,1)} %up_own.1) | copy-start | bytes 786436
  13.5 31.6 %copy-start.2 = (bf16[1,128,1024]{2,1,0:T(8,128)(2,1)S(1)}, bf16[1,128,1024]{2,1,0:T(8,128)(2,1)}, u32[]{:S(2)}) copy-start(bf16[1,128,1024]{2,1,0:T(8,128)(2,1)} %down_own.1) | copy-start | bytes 786436
  21.2 4.5 %collective-permute-start = (f32[16,1024]{1,0:T(8,128)}, f32[16,1024]{1,0:T(8,128)S(1)}, u32[]{:S(2)}, u32[]{:S(2)}) collective-permute-start(f32[16,1024]{1,0:T(8,128)} %attention.1.own), channel_id=1, source_target_pairs={{0,1},{1,0},{2,3},{3,2},{4,5},{5,4},{6,7},{7,6},{8,9},{9,8},{10,11... | collective-permute-start | bytes 196616 | tf_op jit(solution)/shard_map/ppermute | solution.py:295
  25.7 0.8 copy-start.5
  28.1 33.5 %all-to-all-start = ((bf16[128,16,128]{2,1,0:T(8,128)(2,1)}), bf16[128,16,128]{2,1,0:T(8,128)(2,1)S(1)}, u32[]{:S(2)}, u32[]{:S(2)}) async-start(bf16[128,16,128]{2,1,0:T(8,128)(2,1)} %get-tuple-element.11), calls=%async_computation | async-start | bytes 1048576 | tf_op jit(solution)/shard_map/all_to_all | solution.py:337
  43.8 17.8 %collective-permute-start.7 = (bf16[8,96,512]{2,1,0:T(8,128)(2,1)S(1)}, bf16[8,96,512]{2,1,0:T(8,128)(2,1)S(1)}, u32[]{:S(2)}, u32[]{:S(2)}) collective-permute-start(bf16[8,96,512]{2,1,0:T(8,128)(2,1)S(1)} %pad_maximum_fusion.dense_own), channel_id=1, source_target_pairs={{0,1},{1,0},{2,3},{3,2},{4,5},{5,4},{6,7},{7,6},{8,9},{9,8},{10,11... | collective-permute-start | bytes 2359304 | tf_op jit(solution)/shard_map/ppermute | solution.py:295
  44.5 2.3 %collective-permute-start.1 = (bf16[1,1024,128]{2,1,0:T(8,128)(2,1)S(1)}, bf16[1,1024,128]{2,1,0:T(8,128)(2,1)S(1)}, u32[]{:S(2)}, u32[]{:S(2)}) collective-permute-start(bf16[1,1024,128]{2,1,0:T(8,128)(2,1)S(1)} %copy-done), channel_id=1, source_target_pairs={{0,1},{1,0},{2,3},{3,2},{4,5},{5,4},{6,7},{7,6},{8,9},{9,8},{10,11... | collective-permute-start | bytes 786440 | tf_op jit(solution)/shard_map/ppermute | solution.py:295
  44.7 2.5 %collective-permute-start.2 = (bf16[1,1024,128]{2,1,0:T(8,128)(2,1)S(1)}, bf16[1,1024,128]{2,1,0:T(8,128)(2,1)S(1)}, u32[]{:S(2)}, u32[]{:S(2)}) collective-permute-start(bf16[1,1024,128]{2,1,0:T(8,128)(2,1)S(1)} %copy-done.1), channel_id=1, source_target_pairs={{0,1},{1,0},{2,3},{3,2},{4,5},{5,4},{6,7},{7,6},{8,9},{9,8},{10,11... | collective-permute-start | bytes 786440 | tf_op jit(solution)/shard_map/ppermute | solution.py:295
  45.1 2.5 %collective-permute-start.3 = (bf16[1,128,1024]{2,1,0:T(8,128)(2,1)S(1)}, bf16[1,128,1024]{2,1,0:T(8,128)(2,1)S(1)}, u32[]{:S(2)}, u32[]{:S(2)}) collective-permute-start(bf16[1,128,1024]{2,1,0:T(8,128)(2,1)S(1)} %copy-done.2), channel_id=1, source_target_pairs={{0,1},{1,0},{2,3},{3,2},{4,5},{5,4},{6,7},{7,6},{8,9},{9,8},{10,11... | collective-permute-start | bytes 786440 | tf_op jit(solution)/shard_map/ppermute | solution.py:295
  47.6 0.7 copy-start.3
  61.6 1.0 %copy-start.4 = (bf16[1,128,1024]{2,1,0:T(8,128)(2,1)S(1)}, bf16[1,128,1024]{2,1,0:T(8,128)(2,1)}, u32[]{:S(2)}) copy-start(bf16[1,128,1024]{2,1,0:T(8,128)(2,1)} %copy-done.3) | copy-start | bytes 786436
  88.9 4.9 %collective-permute-start.8 = (f32[16,512]{1,0:T(8,128)S(1)}, f32[16,512]{1,0:T(8,128)S(1)}, u32[]{:S(2)}, u32[]{:S(2)}) collective-permute-start(f32[16,512]{1,0:T(8,128)S(1)} %get-tuple-element.16), channel_id=1, source_target_pairs={{0,1},{1,0},{2,3},{3,2},{4,5},{5,4},{6,7},{7,6},{8,9},{9,8},{10,11... | collective-permute-start | bytes 98312 | tf_op jit(solution)/shard_map/ppermute | solution.py:295

commit v2 on v1

--- a/solution.py
+++ b/solution.py
@@ -25,23 +25,24 @@
     heads = lam.shape[0]
     rows = seqs * heads
     block = span // BLOCKS
+    half_span, half_seqs = span // 2, seqs // 2
     weights = [
         pltpu.make_async_copy(src, dst, wsem.at[i])
         for i, (src, dst) in enumerate(((wk_hbm, wk), (wq_hbm, wq), (wv_hbm, wv), (wo_hbm, wo)))
     ]
     key_copies = [
         pltpu.make_async_copy(
-            keys_hbm.at[:, pl.ds(b * block, block), :], keys.at[:, pl.ds(b * block, block), :], ksem.at[b]
+            keys_hbm.at[:, pl.ds(b * half_span, half_span), :], keys.at[:, pl.ds(b * half_span, half_span), :], ksem.at[b]
         )
-        for b in range(BLOCKS)
+        for b in range(2)
     ]
     value_copies = [
         pltpu.make_async_copy(
-            values_hbm.at[pl.ds(b * 4, 4)], values.at[pl.ds(b * 4, 4)], vsem.at[b]
+            values_hbm.at[pl.ds(b * half_seqs, half_seqs)], values.at[pl.ds(b * half_seqs, half_seqs)], vsem.at[b]
         )
-        for b in range(seqs // 4)
+        for b in range(2)
     ]
-    for copy in weights[:3] + key_copies + value_copies + weights[3:]:
+    for copy in weights[:3] + key_copies:
         copy.start()
 
     resid = tokens[...].astype(F32)
@@ -94,9 +95,13 @@
     new_score = jnp.dot(new_row, query, preferred_element_type=F32)[:1]
     peak = new_score
     for b in range(BLOCKS):
-        key_copies[b].wait()
+        if b * block % half_span == 0:
+            key_copies[b * block // half_span].wait()
         past = jnp.concatenate([keys[s, pl.ds(b * block, block), :] for s in range(seqs)], axis=1)
         score = jnp.dot(past, query, preferred_element_type=F32)
+        if b == 0:
+            for copy in value_copies + weights[3:]:
+                copy.start()
         place = lax.broadcasted_iota(jnp.int32, (block, width), 0) + b * block
         score = jnp.where(place < limit, score, -jnp.inf)
         scores[pl.ds(b * block, block), :] = score
@@ -114,8 +119,8 @@
         group = jnp.zeros((8, width), F32)
         for i in range(pair):
             s = g * pair + i
-            if s % 4 == 0:
-                value_copies[s // 4].wait()
+            if s % half_seqs == 0:
+                value_copies[s // half_seqs].wait()
             own = jnp.dot(weight[g * 8 : g * 8 + 8], values[s], preferred_element_type=F32)
             group = jnp.where(part == i, own, group)
         where = pl.ds(g * 8, 8)
@@ -135,9 +140,11 @@
     smem = pl.BlockSpec(memory_space=pltpu.SMEM)
     vmem = pl.BlockSpec(memory_space=pltpu.VMEM)
     hbm = pl.BlockSpec(memory_space=pltpu.HBM)
+    operands = (lens, lam, tokens, mixer_gain, wq, wk, wv, head_gain, wo, cache_keys, cache_values)
+    operands = [pltpu.with_memory_space_constraint(x, pltpu.HBM) for x in operands]
     return pl.pallas_call(
         attention_body,
-        out_shape=jax.ShapeDtypeStruct((seqs, model_width), F32),
+        out_shape=pltpu.VMEM((seqs, model_width), F32),
         in_specs=[smem, smem, vmem, vmem, hbm, hbm, hbm, vmem, hbm, hbm, hbm],
         out_specs=vmem,
         scratch_shapes=[
@@ -151,16 +158,17 @@
             pltpu.VMEM((span, width), F32),
             pltpu.VMEM((seqs * heads, width), F32),
             pltpu.SemaphoreType.DMA((4,)),
-            pltpu.SemaphoreType.DMA((BLOCKS,)),
-            pltpu.SemaphoreType.DMA((4,)),
+            pltpu.SemaphoreType.DMA((2,)),
+            pltpu.SemaphoreType.DMA((2,)),
         ],
-        compiler_params=pltpu.CompilerParams(vmem_limit_bytes=62 * 1024 * 1024),
+        compiler_params=pltpu.CompilerParams(vmem_limit_bytes=20 * 1024 * 1024),
         cost_estimate=pl.CostEstimate(flops=10**9, bytes_accessed=12 * 1024 * 1024, transcendentals=10**6),
         name="attention",
-    )(lens, lam, tokens, mixer_gain, wq, wk, wv, head_gain, wo, cache_keys, cache_values)
+    )(*operands)
 
 
 EP = ("zh", "zl", "yh", "yl", "xh", "xl")
+CUBE = ("zl", "yl", "xl")
 SMEM = pl.BlockSpec(memory_space=pltpu.SMEM)
 VMEM = pl.BlockSpec(memory_space=pltpu.VMEM)
 
@@ -176,13 +184,6 @@
         cost_estimate=pl.CostEstimate(flops=flops, bytes_accessed=2 * 1024 * 1024, transcendentals=10**5),
         name=name,
     )
-
-
-def pack_body(gate, up, down, out):
-    units = down.shape[0]
-    out[pl.ds(0, units), :] = jnp.transpose(gate[...].astype(F32)).astype(BF16)
-    out[pl.ds(units, units), :] = jnp.transpose(up[...].astype(F32)).astype(BF16)
-    out[pl.ds(2 * units, units), :] = down[...]
 
 
 def mid_body(core, tokens, own, other, channel_gain, ids, shares, branch_gate, send, mid, pick, gate, slab):
@@ -229,8 +230,14 @@
 
 
 def experts_body(
-    core, arrived, gate_own, gate_other, up_own, up_other, down_own, down_other, dense_own, dense_other, out, slab
+    core, arrived, gate_own, gate_other, up_own, up_other, dense_own, dense_other, down_own, down_other, out, slab,
+    downs, sems,
 ):
+    down_copies = [
+        pltpu.make_async_copy(src, downs.at[pl.ds(i, 1)], sems.at[i]) for i, src in enumerate((down_own, down_other))
+    ]
+    for copy in down_copies:
+        copy.start()
     peers, lines, width = arrived.shape
     chunks = lines // 2
     slab[...] = arrived[...].reshape(slab.shape).astype(F32)
@@ -239,11 +246,12 @@
     low, high = jnp.concatenate(tokens[: chunks // 2], axis=1), jnp.concatenate(tokens[chunks // 2 :], axis=1)
     is_first = core[0] == 0
     result = jnp.zeros((peers, chunks * width), F32)
-    for w_gate, w_up, w_down in ((gate_own, up_own, down_own), (gate_other, up_other, down_other)):
+    for i, (w_gate, w_up) in enumerate(((gate_own, up_own), (gate_other, up_other))):
         gate_part = jnp.dot(routed, w_gate[0], preferred_element_type=F32)
         up_part = jnp.dot(routed, w_up[0], preferred_element_type=F32)
         hidden = (jax.nn.silu(gate_part) * up_part).astype(BF16)
-        result = result + jnp.dot(hidden, w_down[0], preferred_element_type=F32)
+        down_copies[i].wait()
+        result = result + jnp.dot(hidden, downs[i], preferred_element_type=F32)
     for k in range(chunks):
         slab[pl.ds(k, peers, stride=lines), :] = result[:, k * width : (k + 1) * width]
 
@@ -309,19 +317,17 @@
     sds = jax.ShapeDtypeStruct
     slab = pltpu.VMEM((peers * lines, width), F32)
 
+    packed = jnp.concatenate([dense_gate.T, dense_up.T, dense_down], axis=0)
+    copies = jnp.broadcast_to(packed[None], (2 ** len(CUBE), *packed.shape))
+    gathered = lax.all_to_all(copies, CUBE, 0, 0, tiled=True)
     gate_other, up_other, down_other = (swap(w, "tp") for w in (expert_gate, expert_up, expert_down))
-    units = dense_down.shape[0]
-    packed = call(pack_body, "pack", sds((3 * units, half), BF16), [VMEM] * 3)(dense_gate, dense_up, dense_down)
-    gathered = packed[None]
-    for axis in ("xl", "yl", "zl"):
-        gathered = jnp.concatenate([gathered, swap(gathered, axis)], axis=0)
-    gathered_other = swap(gathered, "tp")
 
     own = attention(
         seq_lengths, head_lambda, tokens, mixer_gain.reshape(1, -1), query_weight, key_weight, value_weight,
         head_gain.reshape(1, -1), out_weight, cache_keys, cache_values,
     )
     other = swap(own, "tp")
+    gathered_other = swap(gathered, "tp")
     send, mid, pick, gate = call(
         mid_body,
         "mid",
@@ -335,9 +341,14 @@
         [slab],
     )(core, tokens, own, other, channel_gain.reshape(1, -1), expert_ids, expert_shares, branch_gate.reshape(1, -1))
     arrived = lax.all_to_all(send, EP, 0, 0, tiled=True)
-    rows_out = call(experts_body, "experts", sds((peers, lines, width), BF16), [SMEM] + [VMEM] * 9, [slab])(
-        core, arrived, expert_gate, gate_other, expert_up, up_other, expert_down, down_other, gathered, gathered_other
-    )
+    pinned = [pltpu.with_memory_space_constraint(w, pltpu.HBM) for w in (expert_down, down_other)]
+    rows_out = call(
+        experts_body,
+        "experts",
+        sds((peers, lines, width), BF16),
+        [SMEM] + [VMEM] * 7 + [pl.BlockSpec(memory_space=pltpu.HBM)] * 2,
+        [slab, pltpu.VMEM((2, *expert_down.shape[1:]), BF16), pltpu.SemaphoreType.DMA((2,))],
+    )(core, arrived, expert_gate, gate_other, expert_up, up_other, gathered, gathered_other, *pinned)
     returned = lax.all_to_all(rows_out, EP, 0, 0, tiled=True)
     keep, give = call(
         combine_body, "combine", (sds((seqs, half), F32), sds((seqs, half), F32)), [SMEM] + [VMEM] * 4, [slab]

time: 94.9 us -> 85.4 us (0.90)
  waiting for transfers between devices: 22.6 us -> 18.5 us
  local copies, waits for them, and re-layouts: 5.22 us -> 1.18 us
    ppermute x9 -> x6, starting transfers between devices: 14.3 us -> 6.89 us  [swap(): return lax.ppermute(value, axis, [(0, 1), (1, 0)])]
    all_to_all x0 -> x1, starting transfers between devices: none -> 5.67 us  [shards(): gathered = lax.all_to_all(copies, CUBE, 0, 0, tiled=True)]
    ppermute x9 -> x6, waiting for transfers between devices: 9.27 us -> 4.12 us  [swap(): return lax.ppermute(value, axis, [(0, 1), (1, 0)])]
    unnamed x28 -> x18, local copies, waits for them, and re-layouts: 5.22 us -> 0.22 us
    pallas_call x2 -> x1, Pallas kernels: 7.87 us -> 6.22 us  [attention(): pl.pallas_call(attention_body, out_shape=pltpu.VMEM((seqs, model_width),...]
    all_to_all x1, starting transfers between devices: 14.6 us -> 15.9 us  [shards(): arrived = lax.all_to_all(send, EP, 0, 0, tiled=True)]
    pallas_call x1, Pallas kernels: 1.58 us -> 2.72 us  [shards(): call(experts_body, 'experts', sds((peers, lines, width), BF16), [SMEM] +...]
    broadcast_in_dim x0 -> x1, local copies, waits for them, and re-layouts: none -> 0.95 us  [shards(): copies = jnp.broadcast_to(packed[None], (2 ** len(CUBE), *packed.shape))]
  transfers between devices with their start and end apart: 10 -> 8, of which waited for: 8 -> 7; matrix products, arithmetic and copies ran while one was open for 1% -> 0% of each run, Pallas kernels for 10% -> 9%
where the time goes in v2:
time: 85.4 us; the launch traced here: 85.1 us
  starting transfers between devices  28.5 us (33%)
  blocking collectives  24.4 us (29%)
  waiting for transfers between devices  18.5 us (22%)
  Pallas kernels  11 us (13%)
  other arithmetic  1.41 us (2%)
  local copies, waits for them, and re-layouts  1.18 us (1%)
    all_to_all x1, blocking collectives, shards(): returned = lax.all_to_all(rows_out, EP, 0, 0, tiled=True)  24.4 us
    all_to_all x1, starting transfers between devices, shards(): arrived = lax.all_to_all(send, EP, 0, 0, tiled=True)  15.9 us
    all_to_all x1, waiting for transfers between devices, shards(): arrived = lax.all_to_all(send, EP, 0, 0, tiled=True)  14.2 us
    ppermute x6, starting transfers between devices, swap(): return lax.ppermute(value, axis, [(0, 1), (1, 0)])  6.89 us
    pallas_call x1, Pallas kernels, attention(): pl.pallas_call(attention_body, out_shape=pltpu.VMEM((seqs, model_width),...  6.22 us
    all_to_all x1, starting transfers between devices, shards(): gathered = lax.all_to_all(copies, CUBE, 0, 0, tiled=True)  5.67 us
    ppermute x6, waiting for transfers between devices, swap(): return lax.ppermute(value, axis, [(0, 1), (1, 0)])  4.12 us
    pallas_call x1, Pallas kernels, shards(): call(experts_body, 'experts', sds((peers, lines, width), BF16), [SMEM] +...  2.72 us
  transfers between devices with their start and end apart: 8, of which 7 were waited for; matrix products, arithmetic and copies ran while one was open for 0% of the time, Pallas kernels for 9%

profile of v2, /device:TPU:1, one launch (start us, length us, event | category | flops | bytes accessed | tf_op | source)
XLA Modules:
  0.0 85.1 jit_solution(116392783049502100)
XLA Ops:
  0.0 0.8 pad_maximum_fusion
  0.8 1.0 %broadcast_in_dim.2 = bf16[8,96,512]{2,1,0:T(8,128)(2,1)} broadcast(bf16[96,512]{1,0:T(8,128)(2,1)S(1)} %pad_maximum_fusion), dimensions={1,2} | broadcast | bytes 884736 | tf_op jit(solution)/shard_map/broadcast_in_dim | solution.py:321
  1.8 5.7 %all-to-all-start.1 = ((bf16[8,96,512]{2,1,0:T(8,128)(2,1)}), bf16[8,96,512]{2,1,0:T(8,128)(2,1)S(1)}, u32[]{:S(2)}, u32[]{:S(2)}) async-start(bf16[8,96,512]{2,1,0:T(8,128)(2,1)} %broadcast_in_dim.2), calls=%async_computation.1 | async-start | bytes 1572864 | tf_op jit(solution)/shard_map/all_to_all | solution.py:322
  7.4 0.0 copy-start.7
  7.4 0.0 copy-start.6
  7.4 0.0 copy-start.2
  7.5 0.0 copy-start.3
  7.5 0.0 copy-start.4
  7.5 0.0 copy-start
  7.5 0.0 copy-start.1
  7.5 0.0 copy-start.5
  7.5 6.2 %attention.1.own = f32[16,1024]{1,0:T(8,128)S(1)} custom-call(s32[16]{0:T(128)} %lens.1, f32[4]{0:T(128)} %lam.1, bf16[16,1024]{1,0:T(8,128)(2,1)} %tokens.3, f32[1,1024]{1,0:T(1,128)} %bitcast.11, bf16[1024,512]{1,0:T(8,128)(2,1)} %wq_hbm.1, bf16[1024,128]{1,0:T(8,128)(2,1)} %wk_hbm.1, bf16[1024,128]{1,0:T(8,128)(2,1)} %wv_hbm.1, f32[1,128]{1,0:T(1,128)} %bitcast.12, ...), custom_call_target="tpu_custom_call" | custom-call | flops 1000000000 | bytes 12582912 | tf_op jit(solution)/shard_map/attention/pallas_call | solution.py:145
  13.7 1.2 %collective-permute-start = (f32[16,1024]{1,0:T(8,128)S(1)}, f32[16,1024]{1,0:T(8,128)S(1)}, u32[]{:S(2)}, u32[]{:S(2)}) collective-permute-start(f32[16,1024]{1,0:T(8,128)S(1)} %attention.1.own), channel_id=1, source_target_pairs={{0,1},{1,0},{2,3},{3,2},{4,5},{5,4},{6,7},{7,6},{8,9},{9,8},{10,11... | collective-permute-start | bytes 196616 | tf_op jit(solution)/shard_map/ppermute | solution.py:303
  14.9 0.0 copy-done.7
  14.9 0.1 copy.23.shares
  15.0 0.0 copy-done.6
  15.0 0.1 copy.22.ids
  15.1 0.7 collective-permute-done.other
  15.8 0.0 copy-done.2
  15.8 0.0 copy-done.3
  15.8 0.0 copy-done.4
  15.8 1.6 %mid.1 = (bf16[128,16,128]{2,1,0:T(8,128)(2,1)}, bf16[16,1024]{1,0:T(8,128)(2,1)S(1)}, bf16[16,128]{1,0:T(8,128)(2,1)S(1)}, f32[16,128]{1,0:T(8,128)S(1)}) custom-call(s32[1]{0:T(128)} %bitcast.core, bf16[16,1024]{1,0:T(8,128)(2,1)S(1)} %copy-done.2, f32[16,1024]{1,0:T(8,128)S(1)} %attention.1.own, f32[16,1024]{1,0:T(8,128)S(1)} %collective-permute-done.other, ...), custom_call_target="tpu_custom_call" | custom-call | flops 100000000 | bytes 2097152 | tf_op jit(solution)/shard_map/mid/pallas_call | solution.py:331
  17.4 0.2 all-to-all-done.1.dense_own
  17.6 15.9 %all-to-all-start = ((bf16[128,16,128]{2,1,0:T(8,128)(2,1)}), bf16[128,16,128]{2,1,0:T(8,128)(2,1)S(1)}, u32[]{:S(2)}, u32[]{:S(2)}) async-start(bf16[128,16,128]{2,1,0:T(8,128)(2,1)} %get-tuple-element.11), calls=%async_computation | async-start | bytes 1048576 | tf_op jit(solution)/shard_map/all_to_all | solution.py:343
  33.5 1.1 %collective-permute-start.3 = (bf16[8,96,512]{2,1,0:T(8,128)(2,1)S(1)}, bf16[8,96,512]{2,1,0:T(8,128)(2,1)S(1)}, u32[]{:S(2)}, u32[]{:S(2)}) collective-permute-start(bf16[8,96,512]{2,1,0:T(8,128)(2,1)S(1)} %all-to-all-done.1.dense_own), channel_id=1, source_target_pairs={{0,1},{1,0},{2,3},{3,2},{4,5},{5,4},{6,7},{7,6},{8,9},{9,8},{10,11... | collective-permute-start | bytes 2359304 | tf_op jit(solution)/shard_map/ppermute | solution.py:303
  34.6 0.0 copy-done
  34.6 0.1 collective-permute-start.1
  34.7 0.0 copy-done.1
  34.7 0.4 collective-permute-start.2
  35.1 0.0 copy-done.5
  35.1 0.1 collective-permute-start.4
  35.2 1.7 %collective-permute-done.1.gate_other = bf16[1,1024,128]{2,1,0:T(8,128)(2,1)S(1)} collective-permute-done((bf16[1,1024,128]{2,1,0:T(8,128)(2,1)S(1)}, bf16[1,1024,128]{2,1,0:T(8,128)(2,1)S(1)}, u32[]{:S(2)}, u32[]{:S(2)}) %collective-permute-start.1) | collective-permute-done | bytes 262176 | tf_op jit(solution)/shard_map/ppermute | solution.py:303
  36.9 0.4 collective-permute-done.2.up_other
  37.3 0.5 collective-permute-done.4.down_other
  37.8 14.2 %all-to-all-done.arrived = bf16[128,16,128]{2,1,0:T(8,128)(2,1)S(1)} async-done(((bf16[128,16,128]{2,1,0:T(8,128)(2,1)}), bf16[128,16,128]{2,1,0:T(8,128)(2,1)S(1)}, u32[]{:S(2)}, u32[]{:S(2)}) %all-to-all-start) | async-done | bytes 524320 | tf_op jit(solution)/shard_map/all_to_all | solution.py:343
  52.0 0.0 collective-permute-done.3.dense_other
  52.0 2.7 %experts.1 = bf16[128,16,128]{2,1,0:T(8,128)(2,1)S(1)} custom-call(s32[1]{0:T(128)} %bitcast.core, bf16[128,16,128]{2,1,0:T(8,128)(2,1)S(1)} %all-to-all-done.arrived, bf16[1,1024,128]{2,1,0:T(8,128)(2,1)S(1)} %copy-done, bf16[1,1024,128]{2,1,0:T(8,128)(2,1)S(1)} %collective-permute-done.1.gate_other, bf16[1,1024,128]{2,1,0:T(8,128)(2,1)S(1)} %copy-done.1, ...), custom_call_target="tpu_custom_call" | custom-call | flops 100000000 | bytes 2097152 | tf_op jit(solution)/shard_map/experts/pallas_call | solution.py:345
  54.7 24.4 %all_to_all.15.returned = bf16[128,16,128]{2,1,0:T(8,128)(2,1)S(1)} all-to-all(bf16[128,16,128]{2,1,0:T(8,128)(2,1)S(1)} %experts.1), channel_id=1, replica_groups=mesh['zh'=4,'zl'=2,'yh'=2,'yl'=2,'xh'=2,'xl'=2,'tp'=2] {'zh','zl','yh','..., dimensions={0} | all-to-all | bytes 1048576 | tf_op jit(solution)/shard_map/all_to_all | solution.py:352
  79.1 0.5 combine.1
  79.6 4.0 %collective-permute-start.5 = (f32[16,512]{1,0:T(8,128)S(1)}, f32[16,512]{1,0:T(8,128)S(1)}, u32[]{:S(2)}, u32[]{:S(2)}) collective-permute-start(f32[16,512]{1,0:T(8,128)S(1)} %get-tuple-element.16), channel_id=1, source_target_pairs={{0,1},{1,0},{2,3},{3,2},{4,5},{5,4},{6,7},{7,6},{8,9},{9,8},{10,11... | collective-permute-start | bytes 98312 | tf_op jit(solution)/shard_map/ppermute | solution.py:303
  83.6 0.9 %collective-permute-done.5 = f32[16,512]{1,0:T(8,128)S(1)} collective-permute-done((f32[16,512]{1,0:T(8,128)S(1)}, f32[16,512]{1,0:T(8,128)S(1)}, u32[]{:S(2)}, u32[]{:S(2)}) %collective-permute-start.5) | collective-permute-done | bytes 32800 | tf_op jit(solution)/shard_map/ppermute | solution.py:303
  84.5 0.6 add_convert_fusion
Async XLA Ops:
  1.8 15.9 %all-to-all-start.1 = ((bf16[8,96,512]{2,1,0:T(8,128)(2,1)}), bf16[8,96,512]{2,1,0:T(8,128)(2,1)S(1)}, u32[]{:S(2)}, u32[]{:S(2)}) async-start(bf16[8,96,512]{2,1,0:T(8,128)(2,1)} %broadcast_in_dim.2), calls=%async_computation.1 | async-start | bytes 1572864 | tf_op jit(solution)/shard_map/all_to_all | solution.py:322
  7.4 7.5 %copy-start.7 = (bf16[16,6]{0,1:T(8,128)(2,1)S(1)}, bf16[16,6]{0,1:T(8,128)(2,1)}, u32[]{:S(2)}) copy-start(bf16[16,6]{0,1:T(8,128)(2,1)} %param.34) | copy-start | bytes 580
  7.4 7.6 %copy-start.6 = (s32[16,6]{0,1:T(8,128)S(1)}, s32[16,6]{0,1:T(8,128)}, u32[]{:S(2)}) copy-start(s32[16,6]{0,1:T(8,128)} %param.33) | copy-start | bytes 1156
  7.4 8.4 %copy-start.2 = (bf16[16,1024]{1,0:T(8,128)(2,1)S(1)}, bf16[16,1024]{1,0:T(8,128)(2,1)}, u32[]{:S(2)}) copy-start(bf16[16,1024]{1,0:T(8,128)(2,1)} %tokens.3) | copy-start | bytes 98308
  7.5 8.4 %copy-start.3 = (f32[1024]{0:T(1024)S(1)}, f32[1024]{0:T(1024)}, u32[]{:S(2)}) copy-start(f32[1024]{0:T(1024)} %param.32) | copy-start | bytes 12292
  7.5 8.4 %copy-start.4 = (f32[1024]{0:T(1024)S(1)}, f32[1024]{0:T(1024)}, u32[]{:S(2)}) copy-start(f32[1024]{0:T(1024)} %param.41) | copy-start | bytes 12292
  7.5 27.1 %copy-start = (bf16[1,1024,128]{2,1,0:T(8,128)(2,1)S(1)}, bf16[1,1024,128]{2,1,0:T(8,128)(2,1)}, u32[]{:S(2)}) copy-start(bf16[1,1024,128]{2,1,0:T(8,128)(2,1)} %gate_own.1) | copy-start | bytes 786436
  7.5 27.2 %copy-start.1 = (bf16[1,1024,128]{2,1,0:T(8,128)(2,1)S(1)}, bf16[1,1024,128]{2,1,0:T(8,128)(2,1)}, u32[]{:S(2)}) copy-start(bf16[1,1024,128]{2,1,0:T(8,128)(2,1)} %up_own.1) | copy-start | bytes 786436
  7.5 27.6 %copy-start.5 = (bf16[1,128,1024]{2,1,0:T(8,128)(2,1)S(1)}, bf16[1,128,1024]{2,1,0:T(8,128)(2,1)}, u32[]{:S(2)}) copy-start(bf16[1,128,1024]{2,1,0:T(8,128)(2,1)} %down_own.1) | copy-start | bytes 786436
  13.7 2.1 %collective-permute-start = (f32[16,1024]{1,0:T(8,128)S(1)}, f32[16,1024]{1,0:T(8,128)S(1)}, u32[]{:S(2)}, u32[]{:S(2)}) collective-permute-start(f32[16,1024]{1,0:T(8,128)S(1)} %attention.1.own), channel_id=1, source_target_pairs={{0,1},{1,0},{2,3},{3,2},{4,5},{5,4},{6,7},{7,6},{8,9},{9,8},{10,11... | collective-permute-start | bytes 196616 | tf_op jit(solution)/shard_map/ppermute | solution.py:303
  17.6 34.4 %all-to-all-start = ((bf16[128,16,128]{2,1,0:T(8,128)(2,1)}), bf16[128,16,128]{2,1,0:T(8,128)(2,1)S(1)}, u32[]{:S(2)}, u32[]{:S(2)}) async-start(bf16[128,16,128]{2,1,0:T(8,128)(2,1)} %get-tuple-element.11), calls=%async_computation | async-start | bytes 1048576 | tf_op jit(solution)/shard_map/all_to_all | solution.py:343
  33.5 18.5 %collective-permute-start.3 = (bf16[8,96,512]{2,1,0:T(8,128)(2,1)S(1)}, bf16[8,96,512]{2,1,0:T(8,128)(2,1)S(1)}, u32[]{:S(2)}, u32[]{:S(2)}) collective-permute-start(bf16[8,96,512]{2,1,0:T(8,128)(2,1)S(1)} %all-to-all-done.1.dense_own), channel_id=1, source_target_pairs={{0,1},{1,0},{2,3},{3,2},{4,5},{5,4},{6,7},{7,6},{8,9},{9,8},{10,11... | collective-permute-start | bytes 2359304 | tf_op jit(solution)/shard_map/ppermute | solution.py:303
  34.6 2.3 %collective-permute-start.1 = (bf16[1,1024,128]{2,1,0:T(8,128)(2,1)S(1)}, bf16[1,1024,128]{2,1,0:T(8,128)(2,1)S(1)}, u32[]{:S(2)}, u32[]{:S(2)}) collective-permute-start(bf16[1,1024,128]{2,1,0:T(8,128)(2,1)S(1)} %copy-done), channel_id=1, source_target_pairs={{0,1},{1,0},{2,3},{3,2},{4,5},{5,4},{6,7},{7,6},{8,9},{9,8},{10,11... | collective-permute-start | bytes 786440 | tf_op jit(solution)/shard_map/ppermute | solution.py:303
  34.7 2.5 %collective-permute-start.2 = (bf16[1,1024,128]{2,1,0:T(8,128)(2,1)S(1)}, bf16[1,1024,128]{2,1,0:T(8,128)(2,1)S(1)}, u32[]{:S(2)}, u32[]{:S(2)}) collective-permute-start(bf16[1,1024,128]{2,1,0:T(8,128)(2,1)S(1)} %copy-done.1), channel_id=1, source_target_pairs={{0,1},{1,0},{2,3},{3,2},{4,5},{5,4},{6,7},{7,6},{8,9},{9,8},{10,11... | collective-permute-start | bytes 786440 | tf_op jit(solution)/shard_map/ppermute | solution.py:303
  35.1 2.6 %collective-permute-start.4 = (bf16[1,128,1024]{2,1,0:T(8,128)(2,1)S(1)}, bf16[1,128,1024]{2,1,0:T(8,128)(2,1)}, u32[]{:S(2)}, u32[]{:S(2)}) collective-permute-start(bf16[1,128,1024]{2,1,0:T(8,128)(2,1)S(1)} %copy-done.5), channel_id=1, source_target_pairs={{0,1},{1,0},{2,3},{3,2},{4,5},{5,4},{6,7},{7,6},{8,9},{9,8},{10,11... | collective-permute-start | bytes 786440 | tf_op jit(solution)/shard_map/ppermute | solution.py:303
  79.6 4.9 %collective-permute-start.5 = (f32[16,512]{1,0:T(8,128)S(1)}, f32[16,512]{1,0:T(8,128)S(1)}, u32[]{:S(2)}, u32[]{:S(2)}) collective-permute-start(f32[16,512]{1,0:T(8,128)S(1)} %get-tuple-element.16), channel_id=1, source_target_pairs={{0,1},{1,0},{2,3},{3,2},{4,5},{5,4},{6,7},{7,6},{8,9},{9,8},{10,11... | collective-permute-start | bytes 98312 | tf_op jit(solution)/shard_map/ppermute | solution.py:303
